TPU v7x, 32 devices: a whole 2x2x4 slice. The times are simulated.
32 devices in a mesh: sp: 16 (over z, y, x), tp: 2 (over core).
Axes of the slice: x: 2, y: 2, z: 4, core: 2. Of those that a mesh axis runs over, the one named last changes fastest.
Arguments:
- resid: bfloat16 [2048, 2048], P('sp'), may hold values from -6 to 6
- queries: bfloat16 [2048, 1024], P('sp', 'tp'), may hold values from -6 to 6
- keys: bfloat16 [2048, 1024], P('sp', 'tp'), may hold values from -6 to 6
- values: bfloat16 [2048, 2048], P('sp', 'tp'), may hold values from -6 to 6
- decay_pre: float32 [2048, 1024], P('sp', 'tp'), may hold values from -4 to 11.5
- out_gate: bfloat16 [2048, 2048], P('sp', 'tp'), may hold values from -6 to 6
- head_gain: float32 [256], replicated, may hold values from 0.1 to 1.9
- out_proj: bfloat16 [2048, 2048], P('tp'), may hold values from -0.25 to 0.25
- mix_gain: float32 [2048], replicated, may hold values from 0.1 to 1.9
- mix_shift: float32 [2048], replicated, may hold values from -3 to 3
- gate_in: bfloat16 [2048, 5632], P('sp', 'tp'), may hold values from -0.125 to 0.125
- up_in: bfloat16 [2048, 5632], P('sp', 'tp'), may hold values from -0.125 to 0.125
- down_out: bfloat16 [5632, 2048], P('tp', 'sp'), may hold values from -0.25 to 0.25
- out_gain: float32 [2048], replicated, may hold values from 0.1 to 1.9
- out_shift: float32 [2048], replicated, may hold values from -2 to 2
Outputs:
- result: bfloat16 [2048, 2048], P('sp')
All inputs are finite; a program needn't handle non-finite values.
Results may differ from a plain program's by a relative error of at most 0.02.
Values may be sent and summed in bfloat16 or wider, within the bound.
A program may use at most 128 MiB of HBM per device.

v0:
```python
import jax
import jax.numpy as jnp
from jax import lax
from jax.sharding import PartitionSpec as P

HK = 128
HV = 256
SPAN = 64


ALPHA = 2.0**0.25
LN_EPS = 1e-05
RMS_EPS = 1e-06
TAU = 16.0


def entering(array, axis, combine, identity):
    count, place = (lax.axis_size(axis), lax.axis_index(axis))
    everything = jax.tree.map(
        lambda part, kind: lax.all_gather(part.astype(kind), axis),
        array,
        (jnp.bfloat16, jnp.bfloat16),
    )
    start = jax.tree.map(
        lambda part, zero: jnp.broadcast_to(jnp.asarray(zero, part.dtype), part.shape),
        array,
        identity,
    )

    def lap(k, before):
        reached = k < place
        new = combine(
            before, jax.tree.map(lambda part, own: part[k].astype(own.dtype), everything, array)
        )
        return jax.tree.map(lambda a, b: jnp.where(reached, a, b), new, before)

    return lax.fori_loop(0, count, lap, start)


def layer_norm(inputs, gain, shift):
    center = inputs - jnp.mean(inputs, axis=-1, keepdims=True)
    spread = jnp.mean(center * center, axis=-1, keepdims=True)
    return center * lax.rsqrt(spread + LN_EPS) * gain + shift


def combine_states(earlier, later):
    return (earlier[0] * later[0], later[0][..., None] * earlier[1] + later[1])


def mix_tokens(queries, keys, values, decay_pre, out_gate, head_gain):
    tok_rows = queries.shape[0]
    local_heads = queries.shape[1] // HK
    blocks = tok_rows // SPAN
    logdecay = jax.nn.log_sigmoid(decay_pre) / TAU
    scaled_q = queries.astype(jnp.float32).reshape(blocks, SPAN, local_heads, HK) * HK ** (-0.5)
    key_block = keys.astype(jnp.float32).reshape(blocks, SPAN, local_heads, HK)
    value_block = values.astype(jnp.float32).reshape(blocks, SPAN, local_heads, HV)
    cumul = jnp.cumsum(logdecay.reshape(blocks, SPAN, local_heads, HK), axis=1)
    last = cumul[:, -1]
    key_decayed = key_block * jnp.exp(last[:, None] - cumul)
    updates = jnp.einsum(
        "nchk,nchv->nhkv", key_decayed, value_block, precision=lax.Precision.HIGHEST
    )

    def advance(running_state, inputs):
        decay_end, state_increment, current_query = inputs
        running_state = jnp.exp(decay_end)[..., None] * running_state + state_increment
        return (
            running_state,
            jnp.einsum(
                "qpy,pyr->qpr", current_query, running_state, precision=lax.Precision.HIGHEST
            ),
        )

    own_state, local_read = lax.scan(
        advance, jnp.zeros((local_heads, HK, HV), jnp.float32), (last, updates, scaled_q)
    )
    block_ends = jnp.cumsum(last, axis=0)
    own_decay = jnp.exp(block_ends[-1])
    identity = (jnp.ones_like(own_decay), jnp.zeros_like(own_state))
    _, incoming = entering((own_decay, own_state), "sp", combine_states, identity)
    carried = jnp.einsum(
        "xepj,pjw->xepw",
        scaled_q * jnp.exp(block_ends)[:, None],
        incoming,
        precision=lax.Precision.HIGHEST,
    )
    state_readout = (local_read + carried).reshape(tok_rows, local_heads, HV)
    normed = (
        state_readout
        * lax.rsqrt(jnp.mean(state_readout * state_readout, axis=-1, keepdims=True) + RMS_EPS)
        * head_gain
    )
    return (
        normed.reshape(tok_rows, local_heads * HV) * jax.nn.silu(out_gate.astype(jnp.float32))
    ).astype(jnp.bfloat16)


def hidden_by_rows(whole_rows, gate_in, up_in):
    gate = jnp.dot(
        whole_rows,
        lax.all_gather(gate_in, "sp", axis=0, tiled=True),
        preferred_element_type=jnp.float32,
    )
    upward = jnp.dot(
        whole_rows,
        lax.all_gather(up_in, "sp", axis=0, tiled=True),
        preferred_element_type=jnp.float32,
    )
    return (jax.nn.silu(gate) * upward).astype(jnp.bfloat16)


def down_by_columns(hidden, down_out):
    return jnp.dot(
        hidden,
        lax.all_gather(down_out, "sp", axis=1, tiled=True),
        preferred_element_type=jnp.float32,
    )


def body(
    resid,
    queries,
    keys,
    values,
    decay_pre,
    out_gate,
    head_gain,
    out_proj,
    mix_gain,
    mix_shift,
    gate_in,
    up_in,
    down_out,
    out_gain,
    out_shift,
):
    tp_count = lax.axis_size("tp")
    tok_rows = queries.shape[0]
    own_count = tok_rows // tp_count
    gated = mix_tokens(queries, keys, values, decay_pre, out_gate, head_gain)
    mixed = lax.psum_scatter(
        jnp.dot(gated, out_proj, preferred_element_type=jnp.float32).astype(jnp.bfloat16),
        "tp",
        scatter_dimension=0,
        tiled=True,
    ).astype(jnp.float32)
    own_resid = lax.dynamic_slice_in_dim(resid, lax.axis_index("tp") * own_count, own_count, 0)
    mid = layer_norm(ALPHA * own_resid.astype(jnp.float32) + mixed, mix_gain, mix_shift).astype(
        jnp.bfloat16
    )
    whole_rows = lax.all_gather(mid, "tp", axis=0, tiled=True)
    hidden = hidden_by_rows(whole_rows, gate_in, up_in)
    ffn = lax.psum_scatter(
        down_by_columns(hidden, down_out).astype(jnp.bfloat16),
        "tp",
        scatter_dimension=0,
        tiled=True,
    ).astype(jnp.float32)
    finished = layer_norm(ALPHA * mid.astype(jnp.float32) + 0.5 * ffn, out_gain, out_shift).astype(
        jnp.bfloat16
    )
    return lax.all_gather(finished, "tp", axis=0, tiled=True)


def solution(mesh):
    return jax.shard_map(
        body,
        mesh=mesh,
        in_specs=(
            P("sp", None),
            P("sp", "tp"),
            P("sp", "tp"),
            P("sp", "tp"),
            P("sp", "tp"),
            P("sp", "tp"),
            P(),
            P("tp", None),
            P(),
            P(),
            P("sp", "tp"),
            P("sp", "tp"),
            P("tp", "sp"),
            P(),
            P(),
        ),
        out_specs=P("sp", None),
        check_vma=False,
    )
```

profile of v0, /device:TPU:0, one launch (start us, length us, event | category | flops | bytes accessed | tf_op | source)
XLA Modules:
  0.0 625.8 jit_solution(3039727210202333603)
XLA Ops:
  6.5 1.1 fusion.12
  7.9 1.0 reshape.101
  8.9 1.1 reshape.94
  10.0 1.0 reshape.103
  11.1 0.6 fusion.13
  11.9 1.4 while.27
  12.1 0.4 fusion.39
  13.3 0.7 convert_element_type.69
  14.2 42.6 %all_gather.25 = bf16[16,4,128]{2,1,0:T(4,128)(2,1)S(1)} all-gather(bf16[1,4,128]{2,1,0:T(4,128)(2,1)S(1)} %fusion.18), channel_id=1, replica_groups=mesh['sp'=16,'tp'=2] {'sp'}, dimensions={0}, use_global_device_ids=true | all-gather | bytes 17408 | tf_op jit(solution)/shard_map/all_gather | solution.py:20
  56.8 35.8 %all-gather.12.cloned.1.call-done = bf16[64,128,256]{2,1,0:T(8,128)(2,1)} async-done(((bf16[4,128,256]{2,1,0:T(8,128)(2,1)}), bf16[64,128,256]{2,1,0:T(8,128)(2,1)}) %all-gather.12.cloned.1.call-update) | async-done | bytes 4194320 | tf_op jit(solution)/shard_map/all_gather | solution.py:20
  92.5 19.1 %while.28 = (s32[]{:T(128)}, f32[4,128,256]{2,1,0:T(8,128)S(1)}, s32[]{:T(128)}, bf16[16,4,128]{2,1,0:T(4,128)(2,1)S(1)}, bf16[16,4,128,256]{3,2,1,0:T(8,128)(2,1)}, /*index=5*/s32[]{:T(128)}, s32[]{:T(128)}) while((s32[]{:T(128)}, f32[4,128,256]{2,1,0:T(8,128)S(1)}, s32[]{:T(128)}, bf16[16,4,128]{2,1,0:T(4,128)(2,1)S(1)}, ...), condition=%wide.region_5.6_spmd.clone, body=%wide.region_4.5_spmd.clone.sunk | while | flops 655876 | bytes 1315945 | solution.py:37
  92.5 1.1 fusion.40
  93.7 1.2 fusion.40
  94.9 1.2 fusion.40
  96.1 1.2 fusion.40
  97.3 1.2 fusion.40
  98.5 1.2 fusion.40
  99.7 1.2 fusion.40
  100.9 1.2 fusion.40
  102.1 1.2 fusion.40
  103.3 1.2 fusion.40
  104.5 1.2 fusion.40
  105.7 1.2 fusion.40
  106.9 1.2 fusion.40
  108.1 1.2 fusion.40
  109.3 1.2 fusion.40
  110.5 1.2 fusion.40
  111.6 0.6 fusion.23
  113.4 3.8 convolution_convert_fusion.1
  117.3 0.7 all-gather.6.cloned.1.call-update
  118.0 0.5 all-gather.10.cloned.1.call-update
  118.6 0.5 all-gather.8.cloned.1.call-update
  119.2 4.7 reduce-scatter.3.cloned.1.call-done
  123.9 1.1 fusion.8
  125.0 1.2 multiply_reduce_fusion.1
  126.3 1.1 add_convert_fusion.1
  127.4 2.2 all_gather.28
  129.6 139.6 %all-gather.6.cloned.1.call-done = bf16[2048,2816]{1,0:T(8,128)(2,1)} async-done(((bf16[128,2816]{1,0:T(8,128)(2,1)}), bf16[2048,2816]{1,0:T(8,128)(2,1)}) %all-gather.6.cloned.1.call-update) | async-done | bytes 11534352 | tf_op jit(solution)/shard_map/all_gather | solution.py:102
  269.2 6.0 fusion.24
  275.2 176.8 %all-gather.10.cloned.1.call-done = bf16[2816,2048]{1,0:T(8,128)(2,1)} async-done(((bf16[2816,128]{1,0:T(8,128)(2,1)}), bf16[2816,2048]{1,0:T(8,128)(2,1)}) %all-gather.10.cloned.1.call-update) | async-done | bytes 11534352 | tf_op jit(solution)/shard_map/all_gather | solution.py:116
  452.0 142.2 %all-gather.8.cloned.1.call-done = bf16[2048,2816]{1,0:T(8,128)(2,1)} async-done(((bf16[128,2816]{1,0:T(8,128)(2,1)}), bf16[2048,2816]{1,0:T(8,128)(2,1)}) %all-gather.8.cloned.1.call-update) | async-done | bytes 11534352 | tf_op jit(solution)/shard_map/all_gather | solution.py:107
  594.3 11.9 %convolution_convert_fusion = bf16[128,2048]{1,0:T(8,128)(2,1)} fusion(bf16[2816,2048]{1,0:T(8,128)(2,1)} %all-gather.10.cloned.1.call-done, bf16[128,2048]{1,0:T(8,128)(2,1)S(1)} %all_gather.28, bf16[2048,2816]{1,0:T(8,128)(2,1)} %all-gather.8.cloned.1.call-done, f32[128,2816]{1,0:T(8,128)S(1)} %fusion.24), kind=kOutput, calls=%fused_computation.12 | convolution fusion | flops 2955214848 | bytes 25559040 | tf_op jit(solution)/shard_map/dot_general | solution.py:114
  606.2 6.3 %reduce-scatter.5.cloned.1.call-done = bf16[64,2048]{1,0:T(8,128)(2,1)} async-done(((bf16[128,2048]{1,0:T(8,128)(2,1)}), bf16[64,2048]{1,0:T(8,128)(2,1)}) %reduce-scatter.5.cloned.1.call-update) | async-done | bytes 262160 | tf_op jit(solution)/shard_map/reduce_scatter | solution.py:154
  612.4 1.2 fusion.9
  613.6 1.2 multiply_reduce_fusion
  614.8 1.1 add_convert_fusion
  616.0 2.2 all_gather.32
  618.2 0.8 copy.72
  (70 shorter events, 2.7 us)
Async XLA Ops:
  6.5 7.6 %copy-start = (f32[256]{0:T(256)S(1)}, f32[256]{0:T(256)}, u32[]{:S(2)}) copy-start(f32[256]{0:T(256)} %param.25) | copy-start | bytes 3076
  6.5 86.0 %all-gather.12.cloned.1.call-start = ((), (), s32[]{:S(2)}) async-start(), calls=%async_computation.7 | async-start | bytes 4456448 | tf_op jit(solution)/shard_map/all_gather | solution.py:20
  14.0 109.9 %reduce-scatter.3.cloned.1.call-start = ((), (), s32[]{:S(2)}) async-start(), calls=%async_computation.2 | async-start | bytes 786432 | tf_op jit(solution)/shard_map/reduce_scatter | solution.py:142
  111.6 1.7 copy-start.6
  113.3 10.6 %copy-start.1 = (bf16[128,2048]{1,0:T(8,128)(2,1)S(1)}, bf16[128,2048]{1,0:T(8,128)(2,1)}, u32[]{:S(2)}) copy-start(bf16[128,2048]{1,0:T(8,128)(2,1)} %param.19) | copy-start | bytes 1572868
  113.3 12.9 %copy-start.2 = (f32[2048]{0:T(1024)S(1)}, f32[2048]{0:T(1024)}, u32[]{:S(2)}) copy-start(f32[2048]{0:T(1024)} %param.28) | copy-start | bytes 24580
  113.3 12.9 %copy-start.3 = (f32[2048]{0:T(1024)S(1)}, f32[2048]{0:T(1024)}, u32[]{:S(2)}) copy-start(f32[2048]{0:T(1024)} %param.27) | copy-start | bytes 24580
  117.2 152.0 %all-gather.6.cloned.1.call-start = ((), (), s32[]{:S(2)}) async-start(), calls=%async_computation.3 | async-start | bytes 12255232 | tf_op jit(solution)/shard_map/all_gather | solution.py:102
  118.0 334.1 %all-gather.10.cloned.1.call-start = ((), (), s32[]{:S(2)}) async-start(), calls=%async_computation.5 | async-start | bytes 12255232 | tf_op jit(solution)/shard_map/all_gather | solution.py:116
  118.5 475.7 %all-gather.8.cloned.1.call-start = ((), (), s32[]{:S(2)}) async-start(), calls=%async_computation.4 | async-start | bytes 12255232 | tf_op jit(solution)/shard_map/all_gather | solution.py:107
  119.1 493.3 %reduce-scatter.5.cloned.1.call-start = ((), (), s32[]{:S(2)}) async-start(), calls=%async_computation.6 | async-start | bytes 786432 | tf_op jit(solution)/shard_map/reduce_scatter | solution.py:154
  275.2 339.6 %copy-start.4 = (f32[2048]{0:T(1024)S(1)}, f32[2048]{0:T(1024)}, u32[]{:S(2)}) copy-start(f32[2048]{0:T(1024)} %param.33) | copy-start | bytes 24580
  275.2 339.6 %copy-start.5 = (f32[2048]{0:T(1024)S(1)}, f32[2048]{0:T(1024)}, u32[]{:S(2)}) copy-start(f32[2048]{0:T(1024)} %param.32) | copy-start | bytes 24580
Sparse Core Ops, SparseCore 0:
  14.1 78.3 all-gather.11
  117.3 6.5 reduce-scatter.2
  126.7 142.5 all-gather.5
  271.8 180.2 all-gather.9
  454.6 139.5 all-gather.7
  606.3 6.0 reduce-scatter.4
where the time goes:
time: 627 us; the launch traced here: 626 us
  waiting for transfers between devices  507 us (81%)
  blocking collectives  47 us (7%)
  other arithmetic  28.2 us (4%)
  matrix products  23.8 us (4%)
  between operations  13.8 us (2%)
    all_gather x1, waiting for transfers between devices, down_by_columns(): lax.all_gather(down_out, 'sp', axis=1, tiled=True)  177 us
    all_gather x1, waiting for transfers between devices, hidden_by_rows(): lax.all_gather(up_in, 'sp', axis=0, tiled=True)  142 us
    all_gather x1, waiting for transfers between devices, hidden_by_rows(): lax.all_gather(gate_in, 'sp', axis=0, tiled=True)  140 us
    all_gather x1, blocking collectives, entering(): lax.all_gather(part.astype(kind), axis)  42.6 us
    all_gather x1, waiting for transfers between devices, entering(): lax.all_gather(part.astype(kind), axis)  35.8 us
    select_n x16, other arithmetic, lap(): return jax.tree.map(lambda a, b: jnp.where(reached, a, b), new, before)  18.4 us
  transfers between devices with their start and end apart: 6, of which 6 were waited for; matrix products, arithmetic and copies ran while one was open for 2% of the time, Pallas kernels for 0%

commit v1 on v0

--- a/solution.py
+++ b/solution.py
@@ -45,6 +45,30 @@
 
 def combine_states(earlier, later):
     return (earlier[0] * later[0], later[0][..., None] * earlier[1] + later[1])
+
+
+def incoming_state(own_decay, own_state):
+    count = lax.axis_size("sp")
+    rows = own_decay.size
+    if rows % count:
+        identity = (jnp.ones_like(own_decay), jnp.zeros_like(own_state))
+        return entering((own_decay, own_state), "sp", combine_states, identity)[1]
+    width = own_state.shape[-1]
+    decay = own_decay.reshape(count, rows // count, 1)
+    high = decay.astype(jnp.bfloat16)
+    low = (decay - high.astype(jnp.float32)).astype(jnp.bfloat16)
+    sent = jnp.concatenate(
+        [own_state.reshape(count, rows // count, width).astype(jnp.bfloat16), high, low], axis=-1
+    )
+    got = lax.all_to_all(sent, "sp", 0, 0, tiled=True).astype(jnp.float32)
+    states, decays = got[..., :width], got[..., width] + got[..., width + 1]
+    running = jnp.zeros_like(states[0])
+    starts = [running]
+    for k in range(count - 1):
+        running = decays[k][:, None] * running + states[k]
+        starts.append(running)
+    back = lax.all_to_all(jnp.stack(starts).astype(jnp.bfloat16), "sp", 0, 0, tiled=True)
+    return back.reshape(own_state.shape).astype(jnp.float32)
 
 
 def mix_tokens(queries, keys, values, decay_pre, out_gate, head_gain):
@@ -77,8 +101,7 @@
     )
     block_ends = jnp.cumsum(last, axis=0)
     own_decay = jnp.exp(block_ends[-1])
-    identity = (jnp.ones_like(own_decay), jnp.zeros_like(own_state))
-    _, incoming = entering((own_decay, own_state), "sp", combine_states, identity)
+    incoming = incoming_state(own_decay, own_state)
     carried = jnp.einsum(
         "xepj,pjw->xepw",
         scaled_q * jnp.exp(block_ends)[:, None],
@@ -116,6 +139,34 @@
         lax.all_gather(down_out, "sp", axis=1, tiled=True),
         preferred_element_type=jnp.float32,
     )
+
+
+def own_units(gate_in, up_in, down_out):
+    count = lax.axis_size("sp")
+    inner, units = gate_in.shape
+    piece = units // count
+    sent = jnp.concatenate(
+        [
+            gate_in.T.reshape(count, piece, inner),
+            up_in.T.reshape(count, piece, inner),
+            down_out.reshape(count, piece, inner),
+        ],
+        axis=1,
+    )
+    got = lax.all_to_all(sent, "sp", 0, 0, tiled=True)
+    whole = got.transpose(1, 0, 2).reshape(3 * piece, count * inner)
+    return whole[:piece], whole[piece : 2 * piece], whole[2 * piece :]
+
+
+def ffn_by_units(mid, weights):
+    gate_t, up_t, down = weights
+    rows = lax.all_gather(mid, ("sp", "tp"), axis=0, tiled=True)
+    contract = (((1,), (1,)), ((), ()))
+    gate = lax.dot_general(rows, gate_t, contract, preferred_element_type=jnp.float32)
+    upward = lax.dot_general(rows, up_t, contract, preferred_element_type=jnp.float32)
+    hidden = (jax.nn.silu(gate) * upward).astype(jnp.bfloat16)
+    part = jnp.dot(hidden, down, preferred_element_type=jnp.float32).astype(jnp.bfloat16)
+    return lax.psum_scatter(part, ("sp", "tp"), scatter_dimension=0, tiled=True)
 
 
 def body(
@@ -138,6 +189,15 @@
     tp_count = lax.axis_size("tp")
     tok_rows = queries.shape[0]
     own_count = tok_rows // tp_count
+    sp_count = lax.axis_size("sp")
+    units = gate_in.shape[1]
+    by_units = (
+        2 * tok_rows * sp_count < 3 * units
+        and units % sp_count == 0
+        and (units // sp_count) % 16 == 0
+        and gate_in.shape[0] == down_out.shape[1]
+    )
+    weights = own_units(gate_in, up_in, down_out) if by_units else None
     gated = mix_tokens(queries, keys, values, decay_pre, out_gate, head_gain)
     mixed = lax.psum_scatter(
         jnp.dot(gated, out_proj, preferred_element_type=jnp.float32).astype(jnp.bfloat16),
@@ -149,14 +209,17 @@
     mid = layer_norm(ALPHA * own_resid.astype(jnp.float32) + mixed, mix_gain, mix_shift).astype(
         jnp.bfloat16
     )
-    whole_rows = lax.all_gather(mid, "tp", axis=0, tiled=True)
-    hidden = hidden_by_rows(whole_rows, gate_in, up_in)
-    ffn = lax.psum_scatter(
-        down_by_columns(hidden, down_out).astype(jnp.bfloat16),
-        "tp",
-        scatter_dimension=0,
-        tiled=True,
-    ).astype(jnp.float32)
+    if by_units:
+        ffn = ffn_by_units(mid, weights).astype(jnp.float32)
+    else:
+        whole_rows = lax.all_gather(mid, "tp", axis=0, tiled=True)
+        hidden = hidden_by_rows(whole_rows, gate_in, up_in)
+        ffn = lax.psum_scatter(
+            down_by_columns(hidden, down_out).astype(jnp.bfloat16),
+            "tp",
+            scatter_dimension=0,
+            tiled=True,
+        ).astype(jnp.float32)
     finished = layer_norm(ALPHA * mid.astype(jnp.float32) + 0.5 * ffn, out_gain, out_shift).astype(
         jnp.bfloat16
     )

time: 627 us -> 370 us (0.59)
  waiting for transfers between devices: 507 us -> 191 us
  blocking collectives: 47 us -> 85.9 us
  starting transfers between devices: 0.2 us -> 12.1 us
    all_gather x4 -> x1, waiting for transfers between devices: 494 us -> 14.8 us  [ffn_by_units(): rows = lax.all_gather(mid, ('sp', 'tp'), axis=0, tiled=True)]
    reduce_scatter x1, waiting for transfers between devices: 6.26 us -> 149 us  [ffn_by_units(): return lax.psum_scatter(part, ('sp', 'tp'), scatter_dimension=0, tiled=True)]
    all_to_all x0 -> x1, blocking collectives: none -> 83.7 us  [own_units(): got = lax.all_to_all(sent, 'sp', 0, 0, tiled=True)]
    all_gather x2 -> x0, blocking collectives: 44.8 us -> none  [the longest x1 42.6 us: entering(): lax.all_gather(part.astype(kind), axis)]
    all_to_all x0 -> x2, waiting for transfers between devices: none -> 21.2 us  [the longest x1 12 us: incoming_state(): got = lax.all_to_all(sent, 'sp', 0, 0, tiled=True).astype(jnp.float32)]
    unnamed x2 -> x15, other arithmetic: 0.01 us -> 18.7 us
    select_n x16 -> x0, other arithmetic: 18.4 us -> none  [lap(): return jax.tree.map(lambda a, b: jnp.where(reached, a, b), new, before)]
    all_to_all x0 -> x2, starting transfers between devices: none -> 11.9 us  [the longest x1 8.34 us: incoming_state(): got = lax.all_to_all(sent, 'sp', 0, 0, tiled=True).astype(jnp.float32)]
  transfers between devices with their start and end apart: 6 -> 5, of which waited for: 6 -> 5; matrix products, arithmetic and copies ran while one was open for 2% -> 0% of each run, Pallas kernels for 0% -> 0%
where the time goes in v1:
time: 370 us; the launch traced here: 368 us
  waiting for transfers between devices  191 us (52%)
  blocking collectives  85.9 us (23%)
  other arithmetic  31.3 us (8%)
  matrix products  27.3 us (7%)
  between operations  13.5 us (4%)
  starting transfers between devices  12.1 us (3%)
  local copies, waits for them, and re-layouts  6.95 us (2%)
    reduce_scatter x1, waiting for transfers between devices, ffn_by_units(): return lax.psum_scatter(part, ('sp', 'tp'), scatter_dimension=0, tiled=True)  149 us
    all_to_all x1, blocking collectives, own_units(): got = lax.all_to_all(sent, 'sp', 0, 0, tiled=True)  83.7 us
    unnamed x15, other arithmetic  18.7 us
    all_gather x1, waiting for transfers between devices, ffn_by_units(): rows = lax.all_gather(mid, ('sp', 'tp'), axis=0, tiled=True)  14.8 us
    dot_general x1, matrix products, ffn_by_units(): jnp.dot(hidden, down, preferred_element_type=jnp.float32)  14.1 us
    all_to_all x1, waiting for transfers between devices, incoming_state(): got = lax.all_to_all(sent, 'sp', 0, 0, tiled=True).astype(jnp.float32)  12 us
    all_to_all x1, waiting for transfers between devices, incoming_state(): lax.all_to_all(jnp.stack(starts).astype(jnp.bfloat16), 'sp', 0, 0, tiled=...  9.21 us
    all_to_all x1, starting transfers between devices, incoming_state(): got = lax.all_to_all(sent, 'sp', 0, 0, tiled=True).astype(jnp.float32)  8.34 us
  transfers between devices with their start and end apart: 5, of which 5 were waited for; matrix products, arithmetic and copies ran while one was open for 0% of the time, Pallas kernels for 0%

profile of v1, /device:TPU:0, one launch (start us, length us, event | category | flops | bytes accessed | tf_op | source)
XLA Modules:
  0.0 368.3 jit_solution(9330066549806061572)
XLA Ops:
  6.5 1.1 fusion.21
  7.9 1.0 reshape.889
  8.9 1.0 reshape.887
  9.9 1.1 reshape.878
  11.7 0.6 fusion.22
  12.4 1.4 while.13
  12.6 0.4 fusion.45
  13.3 0.4 fusion.45
  13.8 0.9 pad_maximum_fusion.1
  14.7 8.3 %all-to-all-start = ((bf16[16,32,258]{2,1,0:T(8,128)(2,1)}), bf16[16,32,258]{2,1,0:T(8,128)(2,1)S(1)}, u32[]{:S(2)}, u32[]{:S(2)}) async-start(bf16[16,32,258]{2,1,0:T(8,128)(2,1)} %pad_maximum_fusion.1), calls=%async_computation | async-start | bytes 786432 | tf_op jit(solution)/shard_map/all_to_all | solution.py:63
  23.0 0.6 constant_dynamic-update-slice_fusion.15
  23.6 12.0 %all-to-all-done = bf16[16,32,258]{2,1,0:T(8,128)(2,1)S(1)} async-done(((bf16[16,32,258]{2,1,0:T(8,128)(2,1)}), bf16[16,32,258]{2,1,0:T(8,128)(2,1)S(1)}, u32[]{:S(2)}, u32[]{:S(2)}) %all-to-all-start) | async-done | bytes 264224 | tf_op jit(solution)/shard_map/all_to_all | solution.py:63
  35.9 0.4 slice_reduce_fusion
  36.2 0.7 constant_dynamic-update-slice_fusion.14
  36.9 0.7 constant_dynamic-update-slice_fusion.13
  37.6 1.4 constant_dynamic-update-slice_fusion.12
  39.0 1.5 constant_dynamic-update-slice_fusion.11
  40.5 1.4 constant_dynamic-update-slice_fusion.10
  41.9 1.5 constant_dynamic-update-slice_fusion.9
  43.4 1.4 constant_dynamic-update-slice_fusion.8
  44.8 1.4 constant_dynamic-update-slice_fusion.7
  46.3 1.5 constant_dynamic-update-slice_fusion.6
  47.7 1.4 constant_dynamic-update-slice_fusion.5
  49.2 1.4 constant_dynamic-update-slice_fusion.4
  50.6 1.5 constant_dynamic-update-slice_fusion.3
  52.1 1.4 constant_dynamic-update-slice_fusion.2
  53.5 1.5 constant_dynamic-update-slice_fusion.1
  55.0 1.4 constant_dynamic-update-slice_fusion
  56.4 3.6 all-to-all-start.1
  60.1 9.2 %all-to-all-done.1 = bf16[16,32,256]{2,1,0:T(8,128)(2,1)S(1)} async-done(((bf16[16,32,256]{2,1,0:T(8,128)(2,1)}), bf16[16,32,256]{2,1,0:T(8,128)(2,1)S(1)}, u32[]{:S(2)}, u32[]{:S(2)}) %all-to-all-start.1) | async-done | bytes 262176 | tf_op jit(solution)/shard_map/all_to_all | solution.py:70
  69.3 0.4 fusion.34
  70.8 3.9 %convolution_convert_fusion.1 = bf16[128,2048]{1,0:T(8,128)(2,1)} fusion(bf16[1024,2048]{1,0:T(8,128)(2,1)} %param.24, bf16[128,1024]{1,0:T(8,128)(2,1)S(1)} %copy-done.11, f32[128,1024]{1,0:T(8,128)S(1)} %bitcast.89, f32[128,1024]{1,0:T(8,128)S(1)} %bitcast.88, f32[1024]{0:T(1024)S(1)} %bitcast.91), kind=kOutput, calls=%fused_computation.10 | convolution fusion | flops 538312704 | bytes 6033408 | tf_op jit(solution)/shard_map/dot_general | solution.py:203
  74.8 6.0 %reduce-scatter.3.cloned.1.call-done = bf16[64,2048]{1,0:T(8,128)(2,1)} async-done(((bf16[128,2048]{1,0:T(8,128)(2,1)}), bf16[64,2048]{1,0:T(8,128)(2,1)}) %reduce-scatter.3.cloned.1.call-update) | async-done | bytes 262160 | tf_op jit(solution)/shard_map/reduce_scatter | solution.py:202
  80.7 1.1 fusion.17
  81.9 1.2 multiply_reduce_fusion.1
  83.1 1.8 add_convert_fusion.1
  85.0 0.4 copy.78
  85.4 0.4 copy.79
  85.9 83.7 %all_to_all.15 = bf16[16,528,128]{2,1,0:T(8,128)(2,1)S(1)} all-to-all(bf16[16,528,128]{2,1,0:T(8,128)(2,1)S(1)} %pad_maximum_fusion), channel_id=1, replica_groups=mesh['sp'=16,'tp'=2] {'sp'}, dimensions={0} | all-to-all | bytes 4325376 | tf_op jit(solution)/shard_map/all_to_all | solution.py:156
  169.8 14.8 %all-gather.2.cloned.1.call-done = bf16[2048,2048]{1,0:T(8,128)(2,1)} async-done(((bf16[64,2048]{1,0:T(8,128)(2,1)}), bf16[2048,2048]{1,0:T(8,128)(2,1)}) %all-gather.2.cloned.1.call-update) | async-done | bytes 8388624 | tf_op jit(solution)/shard_map/all_gather | solution.py:163
  184.5 7.5 %fusion.8 = f32[2048,176]{0,1:T(8,128)} fusion(bf16[2048,2048]{1,0:T(8,128)(2,1)} %all-gather.2.cloned.1.call-done, bf16[16,22,8,128]{3,2,1,0:T(8,128)(2,1)S(1)} %get-tuple-element.132), kind=kOutput, calls=%fused_computation.17 | convolution fusion | flops 1476395008 | bytes 10551296 | tf_op jit(solution)/shard_map/dot_general | solution.py:165
  192.0 14.1 %convolution_convert_fusion = bf16[2048,2048]{1,0:T(8,128)(2,1)} fusion(bf16[2048,2048]{1,0:T(8,128)(2,1)} %all-gather.2.cloned.1.call-done, f32[2048,176]{0,1:T(8,128)} %fusion.8, bf16[16,22,8,128]{3,2,1,0:T(8,128)(2,1)S(1)} %get-tuple-element.131, bf16[16,22,8,128]{3,2,1,0:T(8,128)(2,1)S(1)} %get-tuple-element.130), kind=kOutput, calls=%fused_computation.7 | convolution fusion | flops 2959147008 | bytes 19660800 | tf_op jit(solution)/shard_map/dot_general | solution.py:168
  206.1 149.2 %reduce-scatter.5.cloned.1.call-done = bf16[64,2048]{1,0:T(8,128)(2,1)} async-done(((bf16[2048,2048]{1,0:T(8,128)(2,1)}), bf16[64,2048]{1,0:T(8,128)(2,1)}) %reduce-scatter.5.cloned.1.call-update) | async-done | bytes 262160 | tf_op jit(solution)/shard_map/reduce_scatter | solution.py:169
  355.3 1.2 fusion.18
  356.4 1.2 multiply_reduce_fusion
  357.7 1.1 add_convert_fusion
  358.8 2.2 all_gather.7
  361.0 0.8 copy.147
  (68 shorter events, 3.1 us)
Async XLA Ops:
  6.5 53.5 %copy-start = (f32[256]{0:T(256)S(1)}, f32[256]{0:T(256)}, u32[]{:S(2)}) copy-start(f32[256]{0:T(256)} %param.23) | copy-start | bytes 3076
  14.7 21.0 %all-to-all-start = ((bf16[16,32,258]{2,1,0:T(8,128)(2,1)}), bf16[16,32,258]{2,1,0:T(8,128)(2,1)S(1)}, u32[]{:S(2)}, u32[]{:S(2)}) async-start(bf16[16,32,258]{2,1,0:T(8,128)(2,1)} %pad_maximum_fusion.1), calls=%async_computation | async-start | bytes 786432 | tf_op jit(solution)/shard_map/all_to_all | solution.py:63
  35.7 1.9 copy-start.2
  46.3 24.5 %copy-start.11 = (bf16[128,1024]{1,0:T(8,128)(2,1)S(1)}, bf16[128,1024]{1,0:T(8,128)(2,1)}, u32[]{:S(2)}) copy-start(bf16[128,1024]{1,0:T(8,128)(2,1)} %param.22) | copy-start | bytes 786436
  56.4 12.9 %all-to-all-start.1 = ((bf16[16,32,256]{2,1,0:T(8,128)(2,1)}), bf16[16,32,256]{2,1,0:T(8,128)(2,1)S(1)}, u32[]{:S(2)}, u32[]{:S(2)}) async-start(bf16[16,32,256]{2,1,0:T(8,128)(2,1)} %constant_dynamic-update-slice_fusion), calls=%async_computation.1 | async-start | bytes 524288 | tf_op jit(solution)/shard_map/all_to_all | solution.py:70
  60.0 20.7 %reduce-scatter.3.cloned.1.call-start = ((), (), s32[]{:S(2)}) async-start(), calls=%async_computation.5 | async-start | bytes 786432 | tf_op jit(solution)/shard_map/reduce_scatter | solution.py:202
  70.6 10.1 %copy-start.3 = (bf16[128,2048]{1,0:T(8,128)(2,1)S(1)}, bf16[128,2048]{1,0:T(8,128)(2,1)}, u32[]{:S(2)}) copy-start(bf16[128,2048]{1,0:T(8,128)(2,1)} %param.17) | copy-start | bytes 1572868
  70.8 12.3 %copy-start.7 = (f32[2048]{0:T(1024)S(1)}, f32[2048]{0:T(1024)}, u32[]{:S(2)}) copy-start(f32[2048]{0:T(1024)} %param.26) | copy-start | bytes 24580
  70.8 12.3 %copy-start.8 = (f32[2048]{0:T(1024)S(1)}, f32[2048]{0:T(1024)}, u32[]{:S(2)}) copy-start(f32[2048]{0:T(1024)} %param.25) | copy-start | bytes 24580
  70.8 14.2 %copy-start.4 = (bf16[128,2816]{1,0:T(8,128)(2,1)S(1)}, bf16[128,2816]{1,0:T(8,128)(2,1)}, u32[]{:S(2)}) copy-start(bf16[128,2816]{1,0:T(8,128)(2,1)} %param.27) | copy-start | bytes 2162692
  70.8 14.6 %copy-start.5 = (bf16[128,2816]{1,0:T(8,128)(2,1)S(1)}, bf16[128,2816]{1,0:T(8,128)(2,1)}, u32[]{:S(2)}) copy-start(bf16[128,2816]{1,0:T(8,128)(2,1)} %param.28) | copy-start | bytes 2162692
  74.7 11.0 %copy-start.6 = (bf16[2816,128]{1,0:T(8,128)(2,1)S(1)}, bf16[2816,128]{1,0:T(8,128)(2,1)}, u32[]{:S(2)}) copy-start(bf16[2816,128]{1,0:T(8,128)(2,1)} %param.29) | copy-start | bytes 2162692
  74.7 109.8 %all-gather.2.cloned.1.call-start = ((), (), s32[]{:S(2)}) async-start(), calls=%async_computation.6 | async-start | bytes 8650752 | tf_op jit(solution)/shard_map/all_gather | solution.py:163
  85.0 270.3 %reduce-scatter.5.cloned.1.call-start = ((), (), s32[]{:S(2)}) async-start(), calls=%async_computation.7 | async-start | bytes 8650752 | tf_op jit(solution)/shard_map/reduce_scatter | solution.py:169
  206.1 149.2 %copy-start.1 = (bf16[64,2048]{1,0:T(8,128)(2,1)S(1)}, bf16[64,2048]{1,0:T(8,128)(2,1)}, u32[]{:S(2)}) copy-start(bf16[64,2048]{1,0:T(8,128)(2,1)} %add_convert_fusion.1) | copy-start | bytes 786436
  206.1 151.6 %copy-start.9 = (f32[2048]{0:T(1024)S(1)}, f32[2048]{0:T(1024)}, u32[]{:S(2)}) copy-start(f32[2048]{0:T(1024)} %param.31) | copy-start | bytes 24580
  206.1 151.6 %copy-start.10 = (f32[2048]{0:T(1024)S(1)}, f32[2048]{0:T(1024)}, u32[]{:S(2)}) copy-start(f32[2048]{0:T(1024)} %param.30) | copy-start | bytes 24580
Sparse Core Ops, SparseCore 0:
  74.9 5.8 reduce-scatter.2
  85.1 99.3 all-gather.1
  206.2 148.9 reduce-scatter.4

commit v2 on v0

--- a/solution.py
+++ b/solution.py
@@ -1,6 +1,10 @@
+import functools
+
 import jax
 import jax.numpy as jnp
 from jax import lax
+from jax.experimental import pallas as pl
+from jax.experimental.pallas import tpu as pltpu
 from jax.sharding import PartitionSpec as P
 
 HK = 128
@@ -12,6 +16,7 @@
 LN_EPS = 1e-05
 RMS_EPS = 1e-06
 TAU = 16.0
+MESH = pl.DeviceIdType.MESH
 
 
 def entering(array, axis, combine, identity):
@@ -45,6 +50,93 @@
 
 def combine_states(earlier, later):
     return (earlier[0] * later[0], later[0][..., None] * earlier[1] + later[1])
+
+
+def incoming_state(own_decay, own_state):
+    count = lax.axis_size("sp")
+    rows = own_decay.size
+    if rows % count or (rows // count) % 16:
+        identity = (jnp.ones_like(own_decay), jnp.zeros_like(own_state))
+        return entering((own_decay, own_state), "sp", combine_states, identity)[1]
+    width = own_state.shape[-1]
+    decay = own_decay.reshape(count, rows // count, 1)
+    high = decay.astype(jnp.bfloat16)
+    low = (decay - high.astype(jnp.float32)).astype(jnp.bfloat16)
+    fill = jnp.zeros((count, rows // count, 126), jnp.bfloat16)
+    sent = jnp.concatenate(
+        [own_state.reshape(count, rows // count, width).astype(jnp.bfloat16), high, low, fill],
+        axis=-1,
+    )
+    back = exchange_states(sent, width)
+    return back.reshape(own_state.shape).astype(jnp.float32)
+
+
+def greet(places):
+    barrier = pltpu.get_barrier_semaphore()
+    for place in places:
+        pl.semaphore_signal(barrier, inc=1, device_id=place, device_id_type=MESH)
+    pl.semaphore_wait(barrier, len(places))
+
+
+def remote(src, dst, send, recv, place):
+    return pltpu.make_async_remote_copy(
+        src_ref=src, dst_ref=dst, send_sem=send, recv_sem=recv, device_id=place, device_id_type=MESH
+    )
+
+
+def states_kernel(count, width, sent, back, got, starts, send1, recv1, send2, recv2, own):
+    me, core = lax.axis_index("sp"), lax.axis_index("tp")
+    others = [((me + j) % count, core) for j in range(1, count)]
+    greet(others)
+    first = []
+    for j, place in enumerate(others, 1):
+        copy = remote(sent.at[place[0]], got.at[me], send1.at[j], recv1.at[j], place)
+        copy.start()
+        first.append(copy)
+    keep = pltpu.make_async_copy(sent.at[me], got.at[me], own.at[0])
+    keep.start()
+    keep.wait()
+    for copy in first:
+        copy.wait_recv()
+    running = jnp.zeros(starts.shape[1:], jnp.float32)
+    for k in range(count):
+        starts[k] = running.astype(starts.dtype)
+        if k < count - 1:
+            piece = got[k].astype(jnp.float32)
+            decay = piece[:, width : width + 1] + piece[:, width + 1 : width + 2]
+            running = decay * running + piece[:, :width]
+    second = []
+    for j, place in enumerate(others, 1):
+        copy = remote(starts.at[place[0]], back.at[me], send2.at[j], recv2.at[j], place)
+        copy.start()
+        second.append(copy)
+    keep = pltpu.make_async_copy(starts.at[me], back.at[me], own.at[1])
+    keep.start()
+    keep.wait()
+    for copy in second:
+        copy.wait_recv()
+    for copy in first + second:
+        copy.wait_send()
+
+
+def exchange_states(sent, width):
+    count, rows, whole = sent.shape
+    return pl.pallas_call(
+        functools.partial(states_kernel, count, width),
+        out_shape=jax.ShapeDtypeStruct((count, rows, width), sent.dtype),
+        in_specs=[pl.BlockSpec(memory_space=pltpu.VMEM)],
+        out_specs=pl.BlockSpec(memory_space=pltpu.VMEM),
+        scratch_shapes=[
+            pltpu.VMEM((count, rows, whole), sent.dtype),
+            pltpu.VMEM((count, rows, width), sent.dtype),
+            pltpu.SemaphoreType.DMA((count,)),
+            pltpu.SemaphoreType.DMA((count,)),
+            pltpu.SemaphoreType.DMA((count,)),
+            pltpu.SemaphoreType.DMA((count,)),
+            pltpu.SemaphoreType.DMA((2,)),
+        ],
+        compiler_params=pltpu.CompilerParams(collective_id=1, has_side_effects=True),
+    )(sent)
 
 
 def mix_tokens(queries, keys, values, decay_pre, out_gate, head_gain):
@@ -77,8 +169,7 @@
     )
     block_ends = jnp.cumsum(last, axis=0)
     own_decay = jnp.exp(block_ends[-1])
-    identity = (jnp.ones_like(own_decay), jnp.zeros_like(own_state))
-    _, incoming = entering((own_decay, own_state), "sp", combine_states, identity)
+    incoming = incoming_state(own_decay, own_state)
     carried = jnp.einsum(
         "xepj,pjw->xepw",
         scaled_q * jnp.exp(block_ends)[:, None],
@@ -116,6 +207,241 @@
         lax.all_gather(down_out, "sp", axis=1, tiled=True),
         preferred_element_type=jnp.float32,
     )
+
+
+def own_units(gate_in, up_in, down_out):
+    count = lax.axis_size("sp")
+    inner, units = gate_in.shape
+    piece = units // count
+    sent = jnp.concatenate(
+        [
+            gate_in.T.reshape(count, piece, inner),
+            up_in.T.reshape(count, piece, inner),
+            down_out.reshape(count, piece, inner),
+        ],
+        axis=1,
+    )
+    return sent
+
+
+def mixer_kernel(
+    count,
+    mid,
+    sent,
+    gain,
+    shift,
+    out,
+    rows,
+    weights,
+    part,
+    twin_in,
+    b_out,
+    b_in,
+    a_out,
+    a_in,
+    z_out,
+    z_in,
+    w_send,
+    w_recv,
+    g_send,
+    g_recv,
+    t_recv,
+    own_sem,
+    s_send,
+    p_send,
+    p_recv,
+    b_recv,
+    a_recv,
+    z_recv,
+    f_sem,
+):
+    me, core = lax.axis_index("sp"), lax.axis_index("tp")
+    deep = count // 4
+    own, inner = mid.shape
+    piece = sent.shape[1] // 3
+    lanes = sent.shape[2]
+    x, y = me % 2, (me // 2) % 2
+    to_x, to_y = 1 - 2 * x, 2 - 4 * y
+    to_a = (1 - core) * to_y + core * to_x
+    to_b = core * to_y + (1 - core) * to_x
+    place_a, place_b = (me + to_a, core), (me + to_b, core)
+    twin = (me, 1 - core)
+    others = [((me + j) % count, core) for j in range(1, count)]
+
+    def spot(k, a, b):
+        return (me + 4 * k) % count + a * to_a + b * to_b
+
+    greet(others + [twin])
+
+    keep = [pltpu.make_async_copy(mid, rows.at[2 * me + core], own_sem.at[0])]
+    columns = pl.ds(pl.multiple_of(me * lanes, lanes), lanes)
+    keep.append(pltpu.make_async_copy(sent.at[me], weights.at[:, columns], own_sem.at[1]))
+    for copy in keep:
+        copy.start()
+
+    sends = []
+
+    def forward(k, a, b, place, slot, recv):
+        block = 2 * spot(k, a, b) + core
+        src = mid if (k, a, b) == (0, 0, 0) else rows.at[block]
+        copy = remote(src, rows.at[block], g_send.at[len(sends)], recv.at[slot], place)
+        copy.start()
+        sends.append(copy)
+
+    def index(k, a, b):
+        return (k * 2 + a) * 2 + b
+
+    def landed(k, a, b):
+        block = rows.at[2 * spot(k, a, b) + core]
+        remote(block, block, g_send.at[0], g_recv.at[index(k, a, b)], twin).wait_recv()
+
+    def onward(k, a, b):
+        if not b:
+            if not a:
+                forward(k, 0, 0, place_a, index(k, 1, 0), g_recv)
+            forward(k, a, 0, place_b, index(k, a, 1), g_recv)
+        forward(k, a, b, twin, index(k, b, a), t_recv)
+
+    for k in range(1, deep):
+        forward(0, 0, 0, ((me + 4 * k) % count, core), index(deep - k, 0, 0), g_recv)
+    onward(0, 0, 0)
+    moved = []
+    for j, place in enumerate(others, 1):
+        copy = remote(sent.at[place[0]], weights.at[:, columns], w_send.at[j], w_recv.at[j], place)
+        copy.start()
+        moved.append(copy)
+    order = [(0, 1, 0)] + [(k, 0, 0) for k in range(1, deep)]
+    order += [(k, 1, 0) for k in range(1, deep)]
+    order += [(k, a, 1) for k in range(deep) for a in range(2)]
+    for block in order:
+        landed(*block)
+        onward(*block)
+    for k in range(deep):
+        for a in range(2):
+            for b in range(2):
+                block = rows.at[2 * spot(k, b, a) + 1 - core]
+                remote(block, block, g_send.at[0], t_recv.at[index(k, a, b)], twin).wait_recv()
+    for copy in keep:
+        copy.wait()
+    for copy in moved:
+        copy.wait_recv()
+    for copy in sends + moved:
+        copy.wait_send()
+
+    contract = (((1,), (1,)), ((), ()))
+
+    def to_twin(place):
+        return remote(
+            part.at[2 * place + 1 - core],
+            twin_in.at[place],
+            p_send.at[place],
+            p_recv.at[place],
+            twin,
+        )
+
+    def tile(i, carry):
+        left = rows[pl.ds(4 * i, 4)].reshape(4 * own, inner)
+        gate = lax.dot_general(left, weights[:piece], contract, preferred_element_type=jnp.float32)
+        up = lax.dot_general(
+            left, weights[piece : 2 * piece], contract, preferred_element_type=jnp.float32
+        )
+        hidden = (gate * jax.nn.sigmoid(gate) * up).astype(jnp.bfloat16)
+        down = jnp.dot(hidden, weights[2 * piece :], preferred_element_type=jnp.float32)
+        part[pl.ds(4 * i, 4)] = down.astype(jnp.bfloat16).reshape(4, own, inner)
+        to_twin(2 * i).start()
+        to_twin(2 * i + 1).start()
+        return carry
+
+    lax.fori_loop(0, count // 2, tile, 0)
+
+    def summed(k, a, b, arrived):
+        place = spot(k, a, b)
+        to_twin(place).wait_recv()
+        total = part[2 * place + core].astype(jnp.float32) + twin_in[place].astype(jnp.float32)
+        for ref, sem, slot in arrived:
+            remote(ref.at[slot], ref.at[slot], s_send.at[0], sem.at[slot], twin).wait_recv()
+            total = total + ref[slot].astype(jnp.float32)
+        return total
+
+    pushed = []
+
+    def push(src, dst, recv, slot, place):
+        copy = remote(src.at[slot], dst.at[slot], s_send.at[len(pushed)], recv.at[slot], place)
+        copy.start()
+        pushed.append(copy)
+
+    turn = [k for k in range(1, deep)] + [0]
+    for a in (1, 0):
+        for k in turn:
+            slot = 2 * k + a
+            b_out[slot] = summed(k, a, 1, []).astype(jnp.bfloat16)
+            push(b_out, b_in, b_recv, slot, place_b)
+    for k in turn:
+        a_out[k] = summed(k, 1, 0, [(b_in, b_recv, 2 * k + 1)]).astype(jnp.bfloat16)
+        push(a_out, a_in, a_recv, k, place_a)
+    for k in range(1, deep):
+        z_out[k] = summed(k, 0, 0, [(b_in, b_recv, 2 * k), (a_in, a_recv, k)]).astype(jnp.bfloat16)
+        push(z_out, z_in, z_recv, k, ((me + 4 * k) % count, core))
+    arrived = [(b_in, b_recv, 0), (a_in, a_recv, 0)] + [(z_in, z_recv, k) for k in range(1, deep)]
+    ffn = summed(0, 0, 0, arrived)
+    finished = layer_norm(
+        ALPHA * mid[...].astype(jnp.float32) + 0.5 * ffn, gain[...], shift[...]
+    )
+    out[core] = finished.astype(jnp.bfloat16)
+    last = remote(out.at[core], out.at[core], f_sem.at[0], f_sem.at[1], twin)
+    last.start()
+
+    def drained(place, carry):
+        to_twin(place).wait_send()
+        return carry
+
+    lax.fori_loop(0, count, drained, 0)
+    for copy in pushed:
+        copy.wait_send()
+    last.wait()
+
+
+def mixer(mid, sent, gain, shift):
+    count = lax.axis_size("sp")
+    own, inner = mid.shape
+    deep = count // 4
+    dma = pltpu.SemaphoreType.DMA
+    block = lambda *lead: pltpu.VMEM((*lead, own, inner), jnp.bfloat16)
+    out = pl.pallas_call(
+        functools.partial(mixer_kernel, count),
+        out_shape=jax.ShapeDtypeStruct((2, own, inner), jnp.bfloat16),
+        in_specs=[pl.BlockSpec(memory_space=pltpu.VMEM)] * 4,
+        out_specs=pl.BlockSpec(memory_space=pltpu.VMEM),
+        scratch_shapes=[
+            block(2 * count),
+            pltpu.VMEM((sent.shape[1], inner), jnp.bfloat16),
+            block(2 * count),
+            block(count),
+            block(2 * deep),
+            block(2 * deep),
+            block(deep),
+            block(deep),
+            block(deep),
+            block(deep),
+            dma((count,)),
+            dma((count,)),
+            dma((2 * count,)),
+            dma((count,)),
+            dma((count,)),
+            dma((2,)),
+            dma((count,)),
+            dma((count,)),
+            dma((count,)),
+            dma((2 * deep,)),
+            dma((deep,)),
+            dma((deep,)),
+            dma((2,)),
+        ],
+        compiler_params=pltpu.CompilerParams(
+            collective_id=2, has_side_effects=True, vmem_limit_bytes=60 * 1024 * 1024
+        ),
+    )(mid, sent, gain[None], shift[None])
+    return out.reshape(2 * own, inner)
 
 
 def body(
@@ -138,6 +464,18 @@
     tp_count = lax.axis_size("tp")
     tok_rows = queries.shape[0]
     own_count = tok_rows // tp_count
+    sp_count = lax.axis_size("sp")
+    units = gate_in.shape[1]
+    by_units = (
+        2 * tok_rows * sp_count < 3 * units
+        and units % sp_count == 0
+        and (units // sp_count) % 16 == 0
+        and gate_in.shape[0] == down_out.shape[1]
+        and tp_count == 2
+        and sp_count % 4 == 0
+        and own_count % 16 == 0
+    )
+    weights = own_units(gate_in, up_in, down_out) if by_units else None
     gated = mix_tokens(queries, keys, values, decay_pre, out_gate, head_gain)
     mixed = lax.psum_scatter(
         jnp.dot(gated, out_proj, preferred_element_type=jnp.float32).astype(jnp.bfloat16),
@@ -149,6 +487,8 @@
     mid = layer_norm(ALPHA * own_resid.astype(jnp.float32) + mixed, mix_gain, mix_shift).astype(
         jnp.bfloat16
     )
+    if by_units:
+        return mixer(mid, weights, out_gain, out_shift)
     whole_rows = lax.all_gather(mid, "tp", axis=0, tiled=True)
     hidden = hidden_by_rows(whole_rows, gate_in, up_in)
     ffn = lax.psum_scatter(

time: 627 us -> 210 us (0.33)
  waiting for transfers between devices: 507 us -> 6.25 us
  Pallas kernels: 0 us -> 166 us
  blocking collectives: 47 us -> 0 us
  other arithmetic: 28.2 us -> 8.51 us
  matrix products: 23.8 us -> 6.72 us
    all_gather x4 -> x0, waiting for transfers between devices: 494 us -> none  [the longest x1 177 us: down_by_columns(): lax.all_gather(down_out, 'sp', axis=1, tiled=True)]
    pallas_call x0 -> x2, Pallas kernels: none -> 166 us  [the longest x1 141 us: mixer(): pl.pallas_call(functools.partial(mixer_kernel, count), out_shape=jax.Shap...]
    all_gather x3 -> x0, blocking collectives: 47 us -> none  [the longest x1 42.6 us: entering(): lax.all_gather(part.astype(kind), axis)]
    select_n x16 -> x0, other arithmetic: 18.4 us -> none  [lap(): return jax.tree.map(lambda a, b: jnp.where(reached, a, b), new, before)]
    dot_general x2 -> x0, matrix products: 17.9 us -> none  [the longest x1 11.9 us: down_by_columns(): jnp.dot(hidden, lax.all_gather(down_out, 'sp', axis=1, tiled=True), prefe...]
  transfers between devices with their start and end apart: 6 -> 1, of which waited for: 6 -> 1; matrix products, arithmetic and copies ran while one was open for 2% -> 1% of each run, Pallas kernels for 0% -> 0%
where the time goes in v2:
time: 210 us; the launch traced here: 209 us
  Pallas kernels  166 us (79%)
  between operations  13.7 us (7%)
  other arithmetic  8.51 us (4%)
  local copies, waits for them, and re-layouts  7.5 us (4%)
  matrix products  6.72 us (3%)
  waiting for transfers between devices  6.25 us (3%)
    pallas_call x1, Pallas kernels, mixer(): pl.pallas_call(functools.partial(mixer_kernel, count), out_shape=jax.Shap...  141 us
    pallas_call x1, Pallas kernels, exchange_states(): pl.pallas_call(functools.partial(states_kernel, count, width), out_shape=...  25.7 us
    reduce_scatter x1, waiting for transfers between devices, body(): lax.psum_scatter(jnp.dot(gated, out_proj, preferred_element_type=jnp.floa...  6.23 us
  transfers between devices with their start and end apart: 1, of which 1 were waited for; matrix products, arithmetic and copies ran while one was open for 1% of the time, Pallas kernels for 0%

profile of v2, /device:TPU:0, one launch (start us, length us, event | category | flops | bytes accessed | tf_op | source)
XLA Modules:
  0.0 209.3 jit_solution(9669690522352303625)
XLA Ops:
  6.5 0.0 copy-start
  6.5 0.0 reduce-scatter.2.cloned.1.call-start
  6.5 1.1 fusion.9
  7.7 0.1 reshape.120
  7.8 0.1 fusion.17
  7.9 0.1 exp.52
  8.0 0.2 copy.46
  8.2 0.2 copy.47
  8.3 0.2 copy.48
  8.6 1.0 reshape.133
  9.5 1.1 reshape.123
  10.7 1.0 reshape.135
  11.7 0.1 exponential_multiply_fusion
  11.8 0.6 fusion.10
  12.4 0.1 broadcast_multiply_fusion
  12.5 1.4 while.13
  12.6 0.2 bitcast_add_fusion.2
  12.8 0.4 fusion.27
  13.3 0.2 bitcast_add_fusion.2
  13.5 0.4 fusion.27
  14.0 0.1 pad.6.clone
  14.1 0.9 maximum_maximum_fusion.sent
  15.0 25.7 %shard_map.145 = bf16[16,32,256]{2,1,0:T(8,128)(2,1)} custom-call(bf16[16,32,384]{2,1,0:T(8,128)(2,1)} %maximum_maximum_fusion.sent), custom_call_target="tpu_custom_call" | custom-call | tf_op jit(solution)/shard_map/pallas_call | solution.py:124
  40.7 1.3 fusion.18
  42.0 0.2 multiply_reduce_fusion.1
  42.2 0.1 copy.55
  42.3 0.2 mul.103
  42.5 0.1 copy.65
  42.6 0.3 copy.51
  42.9 0.0 copy-start.2
  43.0 0.1 copy.64
  43.1 0.0 copy-done
  43.1 0.0 copy-done.7
  43.1 0.0 copy-start.3
  43.1 0.0 copy-start.4
  43.1 3.9 %convolution_convert_fusion = bf16[128,2048]{1,0:T(8,128)(2,1)} fusion(bf16[1024,2048]{1,0:T(8,128)(2,1)} %param.24, bf16[128,1024]{1,0:T(8,128)(2,1)S(1)} %copy-done.7, f32[128,1024]{1,0:T(8,128)S(1)} %bitcast.73, f32[128,1024]{1,0:T(8,128)S(1)} %bitcast.72, f32[1024]{0:T(1024)S(1)} %bitcast.77), kind=kOutput, calls=%fused_computation.7 | convolution fusion | flops 538312704 | bytes 6033408 | tf_op jit(solution)/shard_map/dot_general | solution.py:481
  47.0 0.0 reduce-scatter.2.cloned.1.call-update
  47.1 0.0 copy-start.5
  47.1 0.0 copy-start.6
  47.1 0.4 copy.54
  47.5 0.4 copy.53
  47.8 1.5 pad_maximum_fusion.sent
  49.3 6.2 %reduce-scatter.2.cloned.1.call-done = bf16[64,2048]{1,0:T(8,128)(2,1)} async-done(((bf16[128,2048]{1,0:T(8,128)(2,1)}), bf16[64,2048]{1,0:T(8,128)(2,1)}) %reduce-scatter.2.cloned.1.call-update) | async-done | bytes 262160 | tf_op jit(solution)/shard_map/reduce_scatter | solution.py:480
  55.6 1.1 fusion.6
  56.7 1.2 multiply_reduce_fusion
  57.9 1.8 add_convert_fusion.mid
  59.7 140.8 %shard_map.146 = bf16[2,64,2048]{2,1,0:T(8,128)(2,1)} custom-call(bf16[64,2048]{1,0:T(8,128)(2,1)} %add_convert_fusion.mid, bf16[16,528,128]{2,1,0:T(8,128)(2,1)} %pad_maximum_fusion.sent, f32[1,2048]{1,0:T(1,128)} %bitcast.75, f32[1,2048]{1,0:T(1,128)} %bitcast.76), custom_call_target="tpu_custom_call" | custom-call | tf_op jit(solution)/shard_map/pallas_call | solution.py:410
  200.6 1.9 copy.86
  (27 shorter events, 0.2 us)
Async XLA Ops:
  6.5 36.5 %copy-start = (f32[256]{0:T(256)S(1)}, f32[256]{0:T(256)}, u32[]{:S(2)}) copy-start(f32[256]{0:T(256)} %param.23) | copy-start | bytes 3076
  6.5 49.0 %reduce-scatter.2.cloned.1.call-start = ((), (), s32[]{:S(2)}) async-start(), calls=%async_computation.1 | async-start | bytes 786432 | tf_op jit(solution)/shard_map/reduce_scatter | solution.py:480
  14.1 29.0 %copy-start.7 = (bf16[128,1024]{1,0:T(8,128)(2,1)S(1)}, bf16[128,1024]{1,0:T(8,128)(2,1)}, u32[]{:S(2)}) copy-start(bf16[128,1024]{1,0:T(8,128)(2,1)} %param.22) | copy-start | bytes 786436
  42.9 4.1 %copy-start.2 = (bf16[128,2816]{1,0:T(8,128)(2,1)S(1)}, bf16[128,2816]{1,0:T(8,128)(2,1)}, u32[]{:S(2)}) copy-start(bf16[128,2816]{1,0:T(8,128)(2,1)} %param.28) | copy-start | bytes 2162692
  43.1 4.4 %copy-start.3 = (bf16[128,2816]{1,0:T(8,128)(2,1)S(1)}, bf16[128,2816]{1,0:T(8,128)(2,1)}, u32[]{:S(2)}) copy-start(bf16[128,2816]{1,0:T(8,128)(2,1)} %param.27) | copy-start | bytes 2162692
  43.1 4.7 %copy-start.4 = (bf16[2816,128]{1,0:T(8,128)(2,1)S(1)}, bf16[2816,128]{1,0:T(8,128)(2,1)}, u32[]{:S(2)}) copy-start(bf16[2816,128]{1,0:T(8,128)(2,1)} %param.29) | copy-start | bytes 2162692
  47.0 8.5 %copy-start.1 = (bf16[128,2048]{1,0:T(8,128)(2,1)S(1)}, bf16[128,2048]{1,0:T(8,128)(2,1)}, u32[]{:S(2)}) copy-start(bf16[128,2048]{1,0:T(8,128)(2,1)} %param.17) | copy-start | bytes 1572868
  47.1 10.9 %copy-start.5 = (f32[2048]{0:T(1024)S(1)}, f32[2048]{0:T(1024)}, u32[]{:S(2)}) copy-start(f32[2048]{0:T(1024)} %param.26) | copy-start | bytes 24580
  47.1 10.8 %copy-start.6 = (f32[2048]{0:T(1024)S(1)}, f32[2048]{0:T(1024)}, u32[]{:S(2)}) copy-start(f32[2048]{0:T(1024)} %param.25) | copy-start | bytes 24580
Sparse Core Ops, SparseCore 0:
  47.2 8.3 reduce-scatter.1

commit v3 on v2

--- a/solution.py
+++ b/solution.py
@@ -52,23 +52,17 @@
     return (earlier[0] * later[0], later[0][..., None] * earlier[1] + later[1])
 
 
-def incoming_state(own_decay, own_state):
+def packed_state(own_decay, own_state):
     count = lax.axis_size("sp")
-    rows = own_decay.size
-    if rows % count or (rows // count) % 16:
-        identity = (jnp.ones_like(own_decay), jnp.zeros_like(own_state))
-        return entering((own_decay, own_state), "sp", combine_states, identity)[1]
-    width = own_state.shape[-1]
+    rows, width = own_decay.size, own_state.shape[-1]
     decay = own_decay.reshape(count, rows // count, 1)
     high = decay.astype(jnp.bfloat16)
     low = (decay - high.astype(jnp.float32)).astype(jnp.bfloat16)
     fill = jnp.zeros((count, rows // count, 126), jnp.bfloat16)
-    sent = jnp.concatenate(
+    return jnp.concatenate(
         [own_state.reshape(count, rows // count, width).astype(jnp.bfloat16), high, low, fill],
         axis=-1,
     )
-    back = exchange_states(sent, width)
-    return back.reshape(own_state.shape).astype(jnp.float32)
 
 
 def greet(places):
@@ -84,62 +78,7 @@
     )
 
 
-def states_kernel(count, width, sent, back, got, starts, send1, recv1, send2, recv2, own):
-    me, core = lax.axis_index("sp"), lax.axis_index("tp")
-    others = [((me + j) % count, core) for j in range(1, count)]
-    greet(others)
-    first = []
-    for j, place in enumerate(others, 1):
-        copy = remote(sent.at[place[0]], got.at[me], send1.at[j], recv1.at[j], place)
-        copy.start()
-        first.append(copy)
-    keep = pltpu.make_async_copy(sent.at[me], got.at[me], own.at[0])
-    keep.start()
-    keep.wait()
-    for copy in first:
-        copy.wait_recv()
-    running = jnp.zeros(starts.shape[1:], jnp.float32)
-    for k in range(count):
-        starts[k] = running.astype(starts.dtype)
-        if k < count - 1:
-            piece = got[k].astype(jnp.float32)
-            decay = piece[:, width : width + 1] + piece[:, width + 1 : width + 2]
-            running = decay * running + piece[:, :width]
-    second = []
-    for j, place in enumerate(others, 1):
-        copy = remote(starts.at[place[0]], back.at[me], send2.at[j], recv2.at[j], place)
-        copy.start()
-        second.append(copy)
-    keep = pltpu.make_async_copy(starts.at[me], back.at[me], own.at[1])
-    keep.start()
-    keep.wait()
-    for copy in second:
-        copy.wait_recv()
-    for copy in first + second:
-        copy.wait_send()
-
-
-def exchange_states(sent, width):
-    count, rows, whole = sent.shape
-    return pl.pallas_call(
-        functools.partial(states_kernel, count, width),
-        out_shape=jax.ShapeDtypeStruct((count, rows, width), sent.dtype),
-        in_specs=[pl.BlockSpec(memory_space=pltpu.VMEM)],
-        out_specs=pl.BlockSpec(memory_space=pltpu.VMEM),
-        scratch_shapes=[
-            pltpu.VMEM((count, rows, whole), sent.dtype),
-            pltpu.VMEM((count, rows, width), sent.dtype),
-            pltpu.SemaphoreType.DMA((count,)),
-            pltpu.SemaphoreType.DMA((count,)),
-            pltpu.SemaphoreType.DMA((count,)),
-            pltpu.SemaphoreType.DMA((count,)),
-            pltpu.SemaphoreType.DMA((2,)),
-        ],
-        compiler_params=pltpu.CompilerParams(collective_id=1, has_side_effects=True),
-    )(sent)
-
-
-def mix_tokens(queries, keys, values, decay_pre, out_gate, head_gain):
+def local_tokens(queries, keys, values, decay_pre):
     tok_rows = queries.shape[0]
     local_heads = queries.shape[1] // HK
     blocks = tok_rows // SPAN
@@ -169,12 +108,17 @@
     )
     block_ends = jnp.cumsum(last, axis=0)
     own_decay = jnp.exp(block_ends[-1])
-    incoming = incoming_state(own_decay, own_state)
+    carry_q = scaled_q * jnp.exp(block_ends)[:, None]
+    return local_read, carry_q, own_decay, own_state
+
+
+def mix_tokens(local_read, carry_q, own_decay, own_state, out_gate, head_gain):
+    blocks, span, local_heads, _ = carry_q.shape
+    tok_rows = blocks * span
+    identity = (jnp.ones_like(own_decay), jnp.zeros_like(own_state))
+    _, incoming = entering((own_decay, own_state), "sp", combine_states, identity)
     carried = jnp.einsum(
-        "xepj,pjw->xepw",
-        scaled_q * jnp.exp(block_ends)[:, None],
-        incoming,
-        precision=lax.Precision.HIGHEST,
+        "xepj,pjw->xepw", carry_q, incoming, precision=lax.Precision.HIGHEST
     )
     state_readout = (local_read + carried).reshape(tok_rows, local_heads, HV)
     normed = (
@@ -224,13 +168,30 @@
     return sent
 
 
-def mixer_kernel(
+def layer_kernel(
     count,
-    mid,
+    width,
+    states,
+    local_read,
+    carry_q,
+    out_gate,
+    head_gain,
+    out_proj,
+    resid,
+    mix_gain,
+    mix_shift,
     sent,
     gain,
     shift,
     out,
+    got,
+    starts,
+    back,
+    proj,
+    gated,
+    mixed,
+    mixed_in,
+    mid,
     rows,
     weights,
     part,
@@ -241,6 +202,11 @@
     a_in,
     z_out,
     z_in,
+    send1,
+    recv1,
+    send2,
+    recv2,
+    m_sem,
     w_send,
     w_recv,
     g_send,
@@ -273,11 +239,72 @@
 
     greet(others + [twin])
 
-    keep = [pltpu.make_async_copy(mid, rows.at[2 * me + core], own_sem.at[0])]
+    moved = []
+    for j, place in enumerate(others, 1):
+        copy = remote(states.at[place[0]], got.at[me], send1.at[j], recv1.at[j], place)
+        copy.start()
+        moved.append(copy)
     columns = pl.ds(pl.multiple_of(me * lanes, lanes), lanes)
-    keep.append(pltpu.make_async_copy(sent.at[me], weights.at[:, columns], own_sem.at[1]))
+    keep = [
+        pltpu.make_async_copy(states.at[me], got.at[me], own_sem.at[0]),
+        pltpu.make_async_copy(out_proj, proj, own_sem.at[1]),
+        pltpu.make_async_copy(sent.at[me], weights.at[:, columns], own_sem.at[2]),
+    ]
     for copy in keep:
         copy.start()
+    keep[0].wait()
+    for copy in moved:
+        copy.wait_recv()
+    running = jnp.zeros(starts.shape[1:], jnp.float32)
+    for k in range(count):
+        starts[k] = running.astype(starts.dtype)
+        if k < count - 1:
+            state = got[k].astype(jnp.float32)
+            decay = state[:, width : width + 1] + state[:, width + 1 : width + 2]
+            running = decay * running + state[:, :width]
+    returned = []
+    for j, place in enumerate(others, 1):
+        copy = remote(starts.at[place[0]], back.at[me], send2.at[j], recv2.at[j], place)
+        copy.start()
+        returned.append(copy)
+    mine = pltpu.make_async_copy(starts.at[me], back.at[me], own_sem.at[3])
+    mine.start()
+    brought = []
+    for j, place in enumerate(others, 1):
+        copy = remote(sent.at[place[0]], weights.at[:, columns], w_send.at[j], w_recv.at[j], place)
+        copy.start()
+        brought.append(copy)
+    mine.wait()
+    for copy in returned:
+        copy.wait_recv()
+
+    heads = gated.shape[1] // width
+    key_width = carry_q.shape[1] // heads
+    each = count // heads
+    for h in range(heads):
+        wide = slice(h * width, (h + 1) * width)
+        incoming = back[h * each : (h + 1) * each].reshape(key_width, width).astype(jnp.float32)
+        read = local_read[:, wide] + jnp.dot(
+            carry_q[:, h * key_width : (h + 1) * key_width],
+            incoming,
+            precision=lax.Precision.HIGHEST,
+            preferred_element_type=jnp.float32,
+        )
+        size = jnp.mean(read * read, axis=-1, keepdims=True)
+        pre = out_gate[:, wide].astype(jnp.float32)
+        normed = read * lax.rsqrt(size + RMS_EPS) * head_gain[...]
+        gated[:, wide] = (normed * (pre * jax.nn.sigmoid(pre))).astype(jnp.bfloat16)
+    keep[1].wait()
+    summed_heads = jnp.dot(gated[...], proj[...], preferred_element_type=jnp.float32)
+    mixed[...] = summed_heads.astype(jnp.bfloat16).reshape(2, own, inner)
+    swap = remote(mixed.at[1 - core], mixed_in, m_sem.at[0], m_sem.at[1], twin)
+    swap.start()
+    swap.wait()
+    total = mixed[core].astype(jnp.float32) + mixed_in[...].astype(jnp.float32)
+    before = ALPHA * resid[core].astype(jnp.float32) + total
+    middle = layer_norm(before, mix_gain[...], mix_shift[...]).astype(jnp.bfloat16)
+    mid[...] = middle
+    rows[2 * me + core] = middle
 
     sends = []
 
@@ -305,11 +332,6 @@
     for k in range(1, deep):
         forward(0, 0, 0, ((me + 4 * k) % count, core), index(deep - k, 0, 0), g_recv)
     onward(0, 0, 0)
-    moved = []
-    for j, place in enumerate(others, 1):
-        copy = remote(sent.at[place[0]], weights.at[:, columns], w_send.at[j], w_recv.at[j], place)
-        copy.start()
-        moved.append(copy)
     order = [(0, 1, 0)] + [(k, 0, 0) for k in range(1, deep)]
     order += [(k, 1, 0) for k in range(1, deep)]
     order += [(k, a, 1) for k in range(deep) for a in range(2)]
@@ -321,11 +343,10 @@
             for b in range(2):
                 block = rows.at[2 * spot(k, b, a) + 1 - core]
                 remote(block, block, g_send.at[0], t_recv.at[index(k, a, b)], twin).wait_recv()
-    for copy in keep:
-        copy.wait()
-    for copy in moved:
+    keep[2].wait()
+    for copy in brought:
         copy.wait_recv()
-    for copy in sends + moved:
+    for copy in sends + moved + returned + brought:
         copy.wait_send()
 
     contract = (((1,), (1,)), ((), ()))
@@ -339,7 +360,8 @@
             twin,
         )
 
-    def tile(i, carry):
+    def tile(step, side):
+        i = 2 * ((me // 4 + step) % deep) + side
         left = rows[pl.ds(4 * i, 4)].reshape(4 * own, inner)
         gate = lax.dot_general(left, weights[:piece], contract, preferred_element_type=jnp.float32)
         up = lax.dot_general(
@@ -350,9 +372,7 @@
         part[pl.ds(4 * i, 4)] = down.astype(jnp.bfloat16).reshape(4, own, inner)
         to_twin(2 * i).start()
         to_twin(2 * i + 1).start()
-        return carry
-
-    lax.fori_loop(0, count // 2, tile, 0)
+        return side
 
     def summed(k, a, b, arrived):
         place = spot(k, a, b)
@@ -372,6 +392,7 @@
 
     turn = [k for k in range(1, deep)] + [0]
     for a in (1, 0):
+        lax.fori_loop(0, deep, tile, a * (1 - y) + (1 - a) * y)
         for k in turn:
             slot = 2 * k + a
             b_out[slot] = summed(k, a, 1, []).astype(jnp.bfloat16)
@@ -401,18 +422,32 @@
     last.wait()
 
 
-def mixer(mid, sent, gain, shift):
+def layer(local, out_gate, head_gain, out_proj, resid, mix_gain, mix_shift, sent, gain, shift):
+    local_read, carry_q, own_decay, own_state = local
     count = lax.axis_size("sp")
-    own, inner = mid.shape
+    tok_rows, inner = resid.shape
+    own = tok_rows // 2
     deep = count // 4
+    states = packed_state(own_decay, own_state)
+    _, slice_rows, wide = states.shape
+    width = own_state.shape[-1]
     dma = pltpu.SemaphoreType.DMA
     block = lambda *lead: pltpu.VMEM((*lead, own, inner), jnp.bfloat16)
+    near, far = pl.BlockSpec(memory_space=pltpu.VMEM), pl.BlockSpec(memory_space=pl.ANY)
     out = pl.pallas_call(
-        functools.partial(mixer_kernel, count),
+        functools.partial(layer_kernel, count, width),
         out_shape=jax.ShapeDtypeStruct((2, own, inner), jnp.bfloat16),
-        in_specs=[pl.BlockSpec(memory_space=pltpu.VMEM)] * 4,
-        out_specs=pl.BlockSpec(memory_space=pltpu.VMEM),
+        in_specs=[near] * 5 + [far] + [near] * 3 + [far] + [near] * 2,
+        out_specs=near,
         scratch_shapes=[
+            pltpu.VMEM((count, slice_rows, wide), jnp.bfloat16),
+            pltpu.VMEM((count, slice_rows, width), jnp.bfloat16),
+            pltpu.VMEM((count, slice_rows, width), jnp.bfloat16),
+            pltpu.VMEM(out_proj.shape, jnp.bfloat16),
+            pltpu.VMEM((tok_rows, out_proj.shape[0]), jnp.bfloat16),
+            block(2),
+            block(),
+            block(),
             block(2 * count),
             pltpu.VMEM((sent.shape[1], inner), jnp.bfloat16),
             block(2 * count),
@@ -425,10 +460,15 @@
             block(deep),
             dma((count,)),
             dma((count,)),
+            dma((count,)),
+            dma((count,)),
+            dma((2,)),
+            dma((count,)),
+            dma((count,)),
             dma((2 * count,)),
             dma((count,)),
             dma((count,)),
-            dma((2,)),
+            dma((4,)),
             dma((count,)),
             dma((count,)),
             dma((count,)),
@@ -440,8 +480,21 @@
         compiler_params=pltpu.CompilerParams(
             collective_id=2, has_side_effects=True, vmem_limit_bytes=60 * 1024 * 1024
         ),
-    )(mid, sent, gain[None], shift[None])
-    return out.reshape(2 * own, inner)
+    )(
+        states,
+        local_read.reshape(tok_rows, -1),
+        carry_q.reshape(tok_rows, -1),
+        out_gate,
+        head_gain[None],
+        out_proj,
+        resid.reshape(2, own, inner),
+        mix_gain[None],
+        mix_shift[None],
+        sent,
+        gain[None],
+        shift[None],
+    )
+    return out.reshape(tok_rows, inner)
 
 
 def body(
@@ -466,6 +519,7 @@
     own_count = tok_rows // tp_count
     sp_count = lax.axis_size("sp")
     units = gate_in.shape[1]
+    key_rows, heads = queries.shape[1], queries.shape[1] // HK
     by_units = (
         2 * tok_rows * sp_count < 3 * units
         and units % sp_count == 0
@@ -474,9 +528,15 @@
         and tp_count == 2
         and sp_count % 4 == 0
         and own_count % 16 == 0
-    )
-    weights = own_units(gate_in, up_in, down_out) if by_units else None
-    gated = mix_tokens(queries, keys, values, decay_pre, out_gate, head_gain)
+        and key_rows % (16 * sp_count) == 0
+        and sp_count % heads == 0
+    )
+    local = local_tokens(queries, keys, values, decay_pre)
+    if by_units:
+        sent = own_units(gate_in, up_in, down_out)
+        norms = (mix_gain, mix_shift, sent, out_gain, out_shift)
+        return layer(local, out_gate, head_gain, out_proj, resid, *norms)
+    gated = mix_tokens(*local, out_gate, head_gain)
     mixed = lax.psum_scatter(
         jnp.dot(gated, out_proj, preferred_element_type=jnp.float32).astype(jnp.bfloat16),
         "tp",
@@ -487,8 +547,6 @@
     mid = layer_norm(ALPHA * own_resid.astype(jnp.float32) + mixed, mix_gain, mix_shift).astype(
         jnp.bfloat16
     )
-    if by_units:
-        return mixer(mid, weights, out_gain, out_shift)
     whole_rows = lax.all_gather(mid, "tp", axis=0, tiled=True)
     hidden = hidden_by_rows(whole_rows, gate_in, up_in)
     ffn = lax.psum_scatter(

time: 210 us -> 188 us (0.90)
  between operations: 13.7 us -> 0.14 us
  waiting for transfers between devices: 6.25 us -> 0 us
  matrix products: 6.72 us -> 1.5 us
  Pallas kernels: 166 us -> 171 us
  other arithmetic: 8.51 us -> 4.89 us
    reduce_scatter x1 -> x0, waiting for transfers between devices: 6.23 us -> none  [body(): lax.psum_scatter(jnp.dot(gated, out_proj, preferred_element_type=jnp.floa...]
    pallas_call x2 -> x1, Pallas kernels: 166 us -> 171 us  [layer(): pl.pallas_call(functools.partial(layer_kernel, count, width), out_shape=j...]
    dot_general x2 -> x1, matrix products: 4.54 us -> 0.63 us  [local_tokens(): jnp.einsum('nchk,nchv->nhkv', key_decayed, value_block, precision=lax.Pre...]
    reduce_sum x3 -> x0, other arithmetic: 2.47 us -> none  [the longest x1 1.18 us: layer_norm(): spread = jnp.mean(center * center, axis=-1, keepdims=True)]
  transfers between devices with their start and end apart: 1 -> 0, of which waited for: 1 -> 0; matrix products, arithmetic and copies ran while one was open for 1% -> 0% of each run, Pallas kernels for 0% -> 0%
where the time goes in v3:
time: 188 us; the launch traced here: 187 us
  Pallas kernels  171 us (91%)
  local copies, waits for them, and re-layouts  9.51 us (5%)
  other arithmetic  4.89 us (3%)
    pallas_call x1, Pallas kernels, layer(): pl.pallas_call(functools.partial(layer_kernel, count, width), out_shape=j...  171 us
    unnamed x10, local copies, waits for them, and re-layouts  3.94 us

profile of v3, /device:TPU:0, one launch (start us, length us, event | category | flops | bytes accessed | tf_op | source)
XLA Modules:
  0.0 187.0 jit_solution(3392480653828097689)
XLA Ops:
  0.0 0.0 copy-start.3
  0.0 0.1 pad.6.clone
  0.1 1.0 reshape.94
  1.1 1.1 reshape.86
  2.2 1.1 fusion.1
  3.3 0.1 reshape.83
  3.4 0.1 fusion.6
  3.5 0.1 exponential_multiply_fusion
  3.7 0.1 exp.48
  3.8 0.2 copy.35
  4.0 0.2 copy.33
  4.1 0.2 copy.34
  4.4 0.0 copy-done.3
  4.4 0.8 convert_multiply_fusion
  5.2 0.1 mul.38
  5.3 0.6 fusion.2
  5.9 0.0 copy-start
  5.9 3.1 %while.13 = (s32[]{:T(128)}, f32[4,128,256]{2,1,0:T(8,128)S(1)}, f32[2,64,4,256]{3,2,1,0:T(4,128)}, f32[2,4,128]{2,1,0:T(4,128)S(1)}, f32[2,4,128,256]{3,2,1,0:T...) while((s32[]{:T(128)}, f32[4,128,256]{2,1,0:T(8,128)S(1)}, ...), condition=%wide.region_2.3_spmd.clone, body=%wide.region_1.2_spmd.clone.sunk | while | flops 101056512 | bytes 3283063 | solution.py:106
  6.0 0.2 bitcast_add_fusion.2
  6.2 0.4 convolution_bitcast_fusion.2
  6.6 0.9 copy_dynamic-update-slice_fusion.2
  7.5 0.2 bitcast_add_fusion.2
  7.7 0.4 convolution_bitcast_fusion.2
  8.2 0.9 copy_dynamic-update-slice_fusion.2
  9.1 0.0 copy-start.1
  9.1 0.0 copy-start.2
  9.1 2.0 %copy.44 = f32[16,8,4,256]{3,1,2,0:T(8,128)} copy(f32[16,8,4,256]{3,2,1,0:T(4,128)} %bitcast.21) | data formatting | bytes 1048576
  11.1 0.9 maximum_maximum_fusion.states
  12.0 0.0 copy-done
  12.0 0.3 copy.37
  12.4 0.0 copy-done.1
  12.4 0.3 copy.38
  12.7 0.0 copy-done.2
  12.7 1.5 pad_maximum_fusion.sent
  14.2 170.9 %shard_map.145 = bf16[2,64,2048]{2,1,0:T(8,128)(2,1)} custom-call(bf16[16,32,384]{2,1,0:T(8,128)(2,1)} %maximum_maximum_fusion.states, f32[128,1024]{1,0:T(8,128)} %bitcast.50, f32[128,512]{1,0:T(8,128)} %get-tuple-element.91.carry_q, bf16[128,1024]{1,0:T(8,128)(2,1)} %out_gate.1, f32[1,256]{1,0:T(1,128)} %bitcast.62, bf16[1024,2048]{1,0:T(8,128)(2,1)} %out_proj.1, ...), custom_call_target="tpu_custom_call" | custom-call | tf_op jit(solution)/shard_map/pallas_call | solution.py:437
  185.1 1.9 %copy.69 = bf16[128,2048]{1,0:T(8,128)(2,1)} copy(bf16[128,2048]{1,0:T(8,128)(2,1)} %bitcast.51) | data formatting | bytes 1048576
  (14 shorter events, 0.2 us)
Async XLA Ops:
  0.0 4.4 %copy-start.3 = (bf16[128,512]{1,0:T(8,128)(2,1)S(1)}, bf16[128,512]{1,0:T(8,128)(2,1)}, u32[]{:S(2)}) copy-start(bf16[128,512]{1,0:T(8,128)(2,1)} %param.18) | copy-start | bytes 393220
  5.9 6.1 %copy-start = (bf16[128,2816]{1,0:T(8,128)(2,1)S(1)}, bf16[128,2816]{1,0:T(8,128)(2,1)}, u32[]{:S(2)}) copy-start(bf16[128,2816]{1,0:T(8,128)(2,1)} %param.27) | copy-start | bytes 2162692
  9.1 3.3 %copy-start.1 = (bf16[128,2816]{1,0:T(8,128)(2,1)S(1)}, bf16[128,2816]{1,0:T(8,128)(2,1)}, u32[]{:S(2)}) copy-start(bf16[128,2816]{1,0:T(8,128)(2,1)} %param.28) | copy-start | bytes 2162692
  9.1 3.7 %copy-start.2 = (bf16[2816,128]{1,0:T(8,128)(2,1)S(1)}, bf16[2816,128]{1,0:T(8,128)(2,1)}, u32[]{:S(2)}) copy-start(bf16[2816,128]{1,0:T(8,128)(2,1)} %param.29) | copy-start | bytes 2162692

commit v4 on v3

--- a/solution.py
+++ b/solution.py
@@ -270,10 +270,22 @@
     mine = pltpu.make_async_copy(starts.at[me], back.at[me], own_sem.at[3])
     mine.start()
     brought = []
-    for j, place in enumerate(others, 1):
-        copy = remote(sent.at[place[0]], weights.at[:, columns], w_send.at[j], w_recv.at[j], place)
-        copy.start()
-        brought.append(copy)
+
+    def bring(first, last):
+        taken = pl.ds(first * piece, (last - first) * piece)
+        for place in others:
+            slot = len(brought)
+            copy = remote(
+                sent.at[place[0], taken],
+                weights.at[taken, columns],
+                w_send.at[slot],
+                w_recv.at[slot],
+                place,
+            )
+            copy.start()
+            brought.append(copy)
+
+    bring(0, 1)
     mine.wait()
     for copy in returned:
         copy.wait_recv()
@@ -332,6 +344,7 @@
     for k in range(1, deep):
         forward(0, 0, 0, ((me + 4 * k) % count, core), index(deep - k, 0, 0), g_recv)
     onward(0, 0, 0)
+    bring(1, 3)
     order = [(0, 1, 0)] + [(k, 0, 0) for k in range(1, deep)]
     order += [(k, 1, 0) for k in range(1, deep)]
     order += [(k, a, 1) for k in range(deep) for a in range(2)]
@@ -463,8 +476,8 @@
             dma((count,)),
             dma((count,)),
             dma((2,)),
-            dma((count,)),
-            dma((count,)),
+            dma((2 * count,)),
+            dma((2 * count,)),
             dma((2 * count,)),
             dma((count,)),
             dma((count,)),

time: 188 us -> 175 us (0.931)
  Pallas kernels: 171 us -> 158 us
    pallas_call x1, Pallas kernels: 171 us -> 158 us  [layer(): pl.pallas_call(functools.partial(layer_kernel, count, width), out_shape=j...]
where the time goes in v4:
time: 175 us; the launch traced here: 174 us
  Pallas kernels  158 us (90%)
  local copies, waits for them, and re-layouts  9.51 us (5%)
  other arithmetic  4.89 us (3%)
    pallas_call x1, Pallas kernels, layer(): pl.pallas_call(functools.partial(layer_kernel, count, width), out_shape=j...  158 us
    unnamed x10, local copies, waits for them, and re-layouts  3.94 us

profile of v4, /device:TPU:0, one launch (start us, length us, event | category | flops | bytes accessed | tf_op | source)
XLA Modules:
  0.0 174.0 jit_solution(12282896593887033297)
XLA Ops:
  0.0 0.0 copy-start.3
  0.0 0.1 pad.6.clone
  0.1 1.0 reshape.94
  1.1 1.1 reshape.86
  2.2 1.1 fusion.1
  3.3 0.1 reshape.83
  3.4 0.1 fusion.6
  3.5 0.1 exponential_multiply_fusion
  3.7 0.1 exp.48
  3.8 0.2 copy.35
  4.0 0.2 copy.33
  4.1 0.2 copy.34
  4.4 0.0 copy-done.3
  4.4 0.8 convert_multiply_fusion
  5.2 0.1 mul.38
  5.3 0.6 fusion.2
  5.9 0.0 copy-start
  5.9 3.1 %while.13 = (s32[]{:T(128)}, f32[4,128,256]{2,1,0:T(8,128)S(1)}, f32[2,64,4,256]{3,2,1,0:T(4,128)}, f32[2,4,128]{2,1,0:T(4,128)S(1)}, f32[2,4,128,256]{3,2,1,0:T...) while((s32[]{:T(128)}, f32[4,128,256]{2,1,0:T(8,128)S(1)}, ...), condition=%wide.region_2.3_spmd.clone, body=%wide.region_1.2_spmd.clone.sunk | while | flops 101056512 | bytes 3283063 | solution.py:106
  6.0 0.2 bitcast_add_fusion.2
  6.2 0.4 convolution_bitcast_fusion.2
  6.6 0.9 copy_dynamic-update-slice_fusion.2
  7.5 0.2 bitcast_add_fusion.2
  7.7 0.4 convolution_bitcast_fusion.2
  8.2 0.9 copy_dynamic-update-slice_fusion.2
  9.1 0.0 copy-start.1
  9.1 0.0 copy-start.2
  9.1 2.0 %copy.44 = f32[16,8,4,256]{3,1,2,0:T(8,128)} copy(f32[16,8,4,256]{3,2,1,0:T(4,128)} %bitcast.21) | data formatting | bytes 1048576
  11.1 0.9 maximum_maximum_fusion.states
  12.0 0.0 copy-done
  12.0 0.3 copy.37
  12.4 0.0 copy-done.1
  12.4 0.3 copy.38
  12.7 0.0 copy-done.2
  12.7 1.5 pad_maximum_fusion.sent
  14.2 157.9 %shard_map.145 = bf16[2,64,2048]{2,1,0:T(8,128)(2,1)} custom-call(bf16[16,32,384]{2,1,0:T(8,128)(2,1)} %maximum_maximum_fusion.states, f32[128,1024]{1,0:T(8,128)} %bitcast.50, f32[128,512]{1,0:T(8,128)} %get-tuple-element.91.carry_q, bf16[128,1024]{1,0:T(8,128)(2,1)} %out_gate.1, f32[1,256]{1,0:T(1,128)} %bitcast.62, bf16[1024,2048]{1,0:T(8,128)(2,1)} %out_proj.1, ...), custom_call_target="tpu_custom_call" | custom-call | tf_op jit(solution)/shard_map/pallas_call | solution.py:450
  172.2 1.9 %copy.69 = bf16[128,2048]{1,0:T(8,128)(2,1)} copy(bf16[128,2048]{1,0:T(8,128)(2,1)} %bitcast.51) | data formatting | bytes 1048576
  (14 shorter events, 0.2 us)
Async XLA Ops:
  0.0 4.4 %copy-start.3 = (bf16[128,512]{1,0:T(8,128)(2,1)S(1)}, bf16[128,512]{1,0:T(8,128)(2,1)}, u32[]{:S(2)}) copy-start(bf16[128,512]{1,0:T(8,128)(2,1)} %param.18) | copy-start | bytes 393220
  5.9 6.1 %copy-start = (bf16[128,2816]{1,0:T(8,128)(2,1)S(1)}, bf16[128,2816]{1,0:T(8,128)(2,1)}, u32[]{:S(2)}) copy-start(bf16[128,2816]{1,0:T(8,128)(2,1)} %param.27) | copy-start | bytes 2162692
  9.1 3.3 %copy-start.1 = (bf16[128,2816]{1,0:T(8,128)(2,1)S(1)}, bf16[128,2816]{1,0:T(8,128)(2,1)}, u32[]{:S(2)}) copy-start(bf16[128,2816]{1,0:T(8,128)(2,1)} %param.28) | copy-start | bytes 2162692
  9.1 3.7 %copy-start.2 = (bf16[2816,128]{1,0:T(8,128)(2,1)S(1)}, bf16[2816,128]{1,0:T(8,128)(2,1)}, u32[]{:S(2)}) copy-start(bf16[2816,128]{1,0:T(8,128)(2,1)} %param.29) | copy-start | bytes 2162692

commit v5 on v4

--- a/solution.py
+++ b/solution.py
@@ -344,13 +344,15 @@
     for k in range(1, deep):
         forward(0, 0, 0, ((me + 4 * k) % count, core), index(deep - k, 0, 0), g_recv)
     onward(0, 0, 0)
-    bring(1, 3)
+    bring(1, 2)
     order = [(0, 1, 0)] + [(k, 0, 0) for k in range(1, deep)]
     order += [(k, 1, 0) for k in range(1, deep)]
     order += [(k, a, 1) for k in range(deep) for a in range(2)]
     for block in order:
         landed(*block)
         onward(*block)
+        if block == (deep - 1, 0, 0):
+            bring(2, 3)
     for k in range(deep):
         for a in range(2):
             for b in range(2):
@@ -476,8 +478,8 @@
             dma((count,)),
             dma((count,)),
             dma((2,)),
-            dma((2 * count,)),
-            dma((2 * count,)),
+            dma((3 * count,)),
+            dma((3 * count,)),
             dma((2 * count,)),
             dma((count,)),
             dma((count,)),

time: 175 us -> 174 us (level); the launches traced: 174 us -> 171 us
  Pallas kernels: 158 us -> 155 us
    pallas_call x1, Pallas kernels: 158 us -> 155 us  [layer(): pl.pallas_call(functools.partial(layer_kernel, count, width), out_shape=j...]
where the time goes in v5:
time: 174 us; the launch traced here: 171 us
  Pallas kernels  155 us (89%)
  local copies, waits for them, and re-layouts  9.51 us (5%)
  other arithmetic  4.89 us (3%)
    pallas_call x1, Pallas kernels, layer(): pl.pallas_call(functools.partial(layer_kernel, count, width), out_shape=j...  155 us
    unnamed x10, local copies, waits for them, and re-layouts  3.94 us

profile of v5, /device:TPU:0, one launch (start us, length us, event | category | flops | bytes accessed | tf_op | source)
XLA Modules:
  0.0 171.0 jit_solution(14063099501469848316)
XLA Ops:
  0.0 0.0 copy-start.3
  0.0 0.1 pad.6.clone
  0.1 1.0 reshape.94
  1.1 1.1 reshape.86
  2.2 1.1 fusion.1
  3.3 0.1 reshape.83
  3.4 0.1 fusion.6
  3.5 0.1 exponential_multiply_fusion
  3.7 0.1 exp.48
  3.8 0.2 copy.35
  4.0 0.2 copy.33
  4.1 0.2 copy.34
  4.4 0.0 copy-done.3
  4.4 0.8 convert_multiply_fusion
  5.2 0.1 mul.38
  5.3 0.6 fusion.2
  5.9 0.0 copy-start
  5.9 3.1 %while.13 = (s32[]{:T(128)}, f32[4,128,256]{2,1,0:T(8,128)S(1)}, f32[2,64,4,256]{3,2,1,0:T(4,128)}, f32[2,4,128]{2,1,0:T(4,128)S(1)}, f32[2,4,128,256]{3,2,1,0:T...) while((s32[]{:T(128)}, f32[4,128,256]{2,1,0:T(8,128)S(1)}, ...), condition=%wide.region_2.3_spmd.clone, body=%wide.region_1.2_spmd.clone.sunk | while | flops 101056512 | bytes 3283063 | solution.py:106
  6.0 0.2 bitcast_add_fusion.2
  6.2 0.4 convolution_bitcast_fusion.2
  6.6 0.9 copy_dynamic-update-slice_fusion.2
  7.5 0.2 bitcast_add_fusion.2
  7.7 0.4 convolution_bitcast_fusion.2
  8.2 0.9 copy_dynamic-update-slice_fusion.2
  9.1 0.0 copy-start.1
  9.1 0.0 copy-start.2
  9.1 2.0 %copy.44 = f32[16,8,4,256]{3,1,2,0:T(8,128)} copy(f32[16,8,4,256]{3,2,1,0:T(4,128)} %bitcast.21) | data formatting | bytes 1048576
  11.1 0.9 maximum_maximum_fusion.states
  12.0 0.0 copy-done
  12.0 0.3 copy.37
  12.4 0.0 copy-done.1
  12.4 0.3 copy.38
  12.7 0.0 copy-done.2
  12.7 1.5 pad_maximum_fusion.sent
  14.2 154.9 %shard_map.145 = bf16[2,64,2048]{2,1,0:T(8,128)(2,1)} custom-call(bf16[16,32,384]{2,1,0:T(8,128)(2,1)} %maximum_maximum_fusion.states, f32[128,1024]{1,0:T(8,128)} %bitcast.50, f32[128,512]{1,0:T(8,128)} %get-tuple-element.91.carry_q, bf16[128,1024]{1,0:T(8,128)(2,1)} %out_gate.1, f32[1,256]{1,0:T(1,128)} %bitcast.62, bf16[1024,2048]{1,0:T(8,128)(2,1)} %out_proj.1, ...), custom_call_target="tpu_custom_call" | custom-call | tf_op jit(solution)/shard_map/pallas_call | solution.py:452
  169.1 1.9 %copy.69 = bf16[128,2048]{1,0:T(8,128)(2,1)} copy(bf16[128,2048]{1,0:T(8,128)(2,1)} %bitcast.51) | data formatting | bytes 1048576
  (14 shorter events, 0.2 us)
Async XLA Ops:
  0.0 4.4 %copy-start.3 = (bf16[128,512]{1,0:T(8,128)(2,1)S(1)}, bf16[128,512]{1,0:T(8,128)(2,1)}, u32[]{:S(2)}) copy-start(bf16[128,512]{1,0:T(8,128)(2,1)} %param.18) | copy-start | bytes 393220
  5.9 6.1 %copy-start = (bf16[128,2816]{1,0:T(8,128)(2,1)S(1)}, bf16[128,2816]{1,0:T(8,128)(2,1)}, u32[]{:S(2)}) copy-start(bf16[128,2816]{1,0:T(8,128)(2,1)} %param.27) | copy-start | bytes 2162692
  9.1 3.3 %copy-start.1 = (bf16[128,2816]{1,0:T(8,128)(2,1)S(1)}, bf16[128,2816]{1,0:T(8,128)(2,1)}, u32[]{:S(2)}) copy-start(bf16[128,2816]{1,0:T(8,128)(2,1)} %param.28) | copy-start | bytes 2162692
  9.1 3.7 %copy-start.2 = (bf16[2816,128]{1,0:T(8,128)(2,1)S(1)}, bf16[2816,128]{1,0:T(8,128)(2,1)}, u32[]{:S(2)}) copy-start(bf16[2816,128]{1,0:T(8,128)(2,1)} %param.29) | copy-start | bytes 2162692
